TPU v7x, 128 devices: a whole 4x4x4 slice. The times are simulated.
128 devices in a mesh: sp: 16 (over z, x), tp: 8 (over y, core).
Axes of the slice: x: 4, y: 4, z: 4, core: 2. Of those that a mesh axis runs over, the one named last changes fastest.
Arguments:
- tokens: bfloat16 [4096, 3072], P('sp', 'tp'), may hold values from -6 to 6
- norm_gain: float32 [3072], replicated, may hold values from 0.1 to 1.9
- state_in_weight: bfloat16 [3072, 1024], P('sp', 'tp'), may hold values from -0.109375 to 0.109375
- pool_in_weight: bfloat16 [3072, 1024], P('sp', 'tp'), may hold values from -0.109375 to 0.109375
- rate_real: float32 [64, 64], replicated, may hold values from -1.5 to -0.5
- rate_imag: float32 [64, 64], replicated, may hold values from 0 to 200
- log_step: float32 [64], replicated, may hold values from -2 to 0.7
- input_real: float32 [64, 64, 16], replicated, may hold values from -1 to 1
- input_imag: float32 [64, 64, 16], replicated, may hold values from -1 to 1
- output_real: float32 [64, 16, 64], replicated, may hold values from -112 to 112
- output_imag: float32 [64, 16, 64], replicated, may hold values from -112 to 112
- skip_gain: float32 [1024], replicated, may hold values from -3 to 3
- pool_weight: bfloat16 [16, 64, 64], replicated, may hold values from -0.75 to 0.75
- pool_gain: float32 [1024], replicated, may hold values from 0.1 to 1.9
- state_out_weight: bfloat16 [1024, 3072], P('sp', 'tp'), may hold values from -0.125 to 0.125
- pool_out_weight: bfloat16 [1024, 3072], P('sp', 'tp'), may hold values from -0.125 to 0.125
Outputs:
- mixer_output: bfloat16 [4096, 3072], P('sp', 'tp')
All inputs are finite; a program needn't handle non-finite values.
Results may differ from a plain program's by a relative error of at most 0.0065.
Values may be sent and summed in bfloat16 or wider, within the bound.
A program may use at most 64 MiB of HBM per device.

v0:
```python
import jax
import jax.numpy as jnp
from jax import lax
from jax.sharding import Mesh
from jax.sharding import PartitionSpec as P

SSM_GROUP = 16
POOL_GROUP = 64
TP = ("tp_0", "tp_1")


epsilon = 1e-06
highest = lax.Precision.HIGHEST
window_reach = 16


def in_one_piece(arrays, axis, dim, along):
    widths = [a.shape[along] for a in arrays]
    both = jnp.concatenate(arrays, axis=along)
    result = lax.all_gather(both, axis, axis=dim, tiled=True)
    return tuple(jnp.split(result, [sum(widths[:k]) for k in range(1, len(widths))], axis=along))


def edges_of(length, count):
    turn = length // count
    if turn >= 8:
        turn -= turn % 8
    return [turn * k for k in range(1, count)]


def stacked_from(array, axes, turns):
    parts = array[None]
    for k in turns:
        parts = lax.all_gather(parts, axes[k], axis=0, tiled=True)
    carried = [lax.axis_size(axes[k]) for k in reversed(turns)]
    parts = parts.reshape(*carried, *array.shape)
    turned = sorted(range(len(turns)), key=lambda place: turns[len(turns) - 1 - place])
    return parts.transpose(*turned, *range(len(turns), parts.ndim)).reshape(-1, *array.shape)


def in_order(parts, dim):
    dims = list(parts.shape[1:])
    dims[dim] *= parts.shape[0]
    return jnp.moveaxis(parts, 0, dim).reshape(dims)


def spread_gather(array, axes, dim):
    widest = max(range(max(1, array.ndim - 1)), key=lambda d: array.shape[d])
    count, gathered = (len(axes), [])
    for first, share in enumerate(
        jnp.split(array, edges_of(array.shape[widest], count), axis=widest)
    ):
        if share.size:
            turns = [(first - k) % count for k in range(count)]
            gathered.append(stacked_from(share, axes, turns))
    return in_order(jnp.concatenate(gathered, axis=widest + 1), dim)


def copy_for_each(array, axis):
    peers = lax.axis_size(axis)
    return lax.all_to_all(
        jnp.broadcast_to(array[None], (peers, *array.shape)), axis, 0, 0, tiled=True
    )


def all_in_one(array, axis):
    leaves = jax.tree.leaves(array)
    turns = sorted(range(len(leaves)), key=lambda k: -leaves[k].size)
    width = (1, *leaves[turns[0]].shape)[-1]
    lines = [
        jnp.pad(leaves[k].reshape(-1), (0, -leaves[k].size % width)).reshape(-1, width)
        for k in turns
    ]
    both, at, found = (copy_for_each(jnp.concatenate(lines), axis), 0, {})
    for k, line in zip(turns, lines):
        share = both[:, at : at + len(line)].reshape(len(both), -1)
        found[k] = share[:, : leaves[k].size].reshape(-1, *leaves[k].shape)
        at += len(line)
    numbers = iter(range(len(leaves)))
    return jax.tree.map(lambda _: found[next(numbers)], array)


def joined_by_halves(pieces, combine):
    while len(jax.tree.leaves(pieces)[0]) > 1:
        pieces = jax.vmap(combine)(
            *(jax.tree.map(lambda part: part[side::2], pieces) for side in (0, 1))
        )
    return jax.tree.map(lambda part: part[0], pieces)


def entering(array, axis, combine, identity):
    peers, position = (lax.axis_size(axis), lax.axis_index(axis))
    passed = jnp.arange(peers) < position

    def kept(part, zero, own):
        part = jnp.where(
            passed.reshape(-1, *(1 for _ in own.shape)), part, jnp.asarray(zero, own.dtype)
        )
        return part

    pieces = all_in_one(array, axis)
    return joined_by_halves(jax.tree.map(kept, pieces, identity, array), combine)


def passed_along(value, axis, steps):
    count = lax.axis_size(axis)
    first, last = (max(0, -steps), min(count, count - steps))
    return lax.ppermute(value, axis, [(source, source + steps) for source in range(first, last)])


def discretize(rate_real, rate_imag, log_step, length):
    step_size = jnp.exp(log_step)[:, None] / length
    exponent = rate_real * step_size
    angle = rate_imag * step_size
    magnitude = jnp.exp(exponent)
    decay_real = magnitude * jnp.cos(angle)
    decay_imag = magnitude * jnp.sin(angle)
    less_one = jnp.expm1(exponent) * jnp.cos(angle) - 2.0 * jnp.square(jnp.sin(0.5 * angle))
    denominator = rate_real * rate_real + rate_imag * rate_imag
    factor_real = (less_one * rate_real + decay_imag * rate_imag) / denominator
    factor_imag = (decay_imag * rate_real - less_one * rate_imag) / denominator
    return (exponent, angle, decay_real, decay_imag, factor_real, factor_imag)


def complex_product(left_pair, right_pair):
    return jnp.stack(
        [
            left_pair[0] * right_pair[0] - left_pair[1] * right_pair[1],
            left_pair[0] * right_pair[1] + left_pair[1] * right_pair[0],
        ]
    )


def scan_combine(first_part, second_part):
    first_decay_real, first_decay_imag, first_real, first_imag = first_part
    second_decay_real, second_decay_imag, second_real, second_imag = second_part
    return (
        first_decay_real * second_decay_real - first_decay_imag * second_decay_imag,
        first_decay_real * second_decay_imag + first_decay_imag * second_decay_real,
        second_decay_real * first_real - second_decay_imag * first_imag + second_real,
        second_decay_real * first_imag + second_decay_imag * first_real + second_imag,
    )


def chain_combine(earlier, later):
    return (complex_product(later[0], earlier[0]), complex_product(later[0], earlier[1]) + later[1])


def local_slice(array, first_index, count_here):
    return lax.dynamic_slice_in_dim(array, first_index, count_here, 0)


def body(
    tokens,
    norm_gain,
    state_in_weight,
    pool_in_weight,
    rate_real,
    rate_imag,
    log_step,
    input_real,
    input_imag,
    output_real,
    output_imag,
    skip_gain,
    pool_weight,
    pool_gain,
    state_out_weight,
    pool_out_weight,
):
    state_in_full, pool_in_full, state_out_full, pool_out_full = (
        *in_one_piece((state_in_weight, pool_in_weight), "sp", 0, 1),
        *in_one_piece((state_out_weight, pool_out_weight), "sp", 0, 1),
    )
    row_count = tokens.shape[0]
    model_width = norm_gain.shape[0]
    state_width = state_in_full.shape[1]
    pool_width = pool_in_full.shape[1]
    features = spread_gather(tokens, TP, 1).astype(jnp.float32)
    scaled = (features * norm_gain).astype(jnp.bfloat16)
    state_rows = state_in_full
    pool_rows = pool_in_full
    state_sum = jnp.dot(scaled, state_rows, preferred_element_type=jnp.float32)
    pool_sum = jnp.dot(scaled, pool_rows, preferred_element_type=jnp.float32)
    squares = jnp.sum(features * features, axis=1)
    state_sum, pool_sum, squares = (state_sum, pool_sum, squares)
    inverse = lax.rsqrt(squares / model_width + epsilon)[:, None]
    state_in = (state_sum * inverse).astype(jnp.bfloat16)
    pool_in = (pool_sum * inverse).astype(jnp.bfloat16)
    head_index = lax.axis_index(TP)
    block_index = lax.axis_index("sp")
    groups_here = state_width // SSM_GROUP
    first_group = head_index * groups_here
    length = row_count * lax.axis_size("sp")
    exponent, angle, decay_real, decay_imag, factor_real, factor_imag = discretize(
        local_slice(rate_real, first_group, groups_here),
        local_slice(rate_imag, first_group, groups_here),
        local_slice(log_step, first_group, groups_here),
        length,
    )
    state_columns = groups_here * decay_real.shape[1]
    exponent = exponent.reshape(state_columns)
    angle = angle.reshape(state_columns)
    decay_real = decay_real.reshape(state_columns)
    decay_imag = decay_imag.reshape(state_columns)
    group_identity = jnp.eye(groups_here, dtype=jnp.float32)
    local_in_real = local_slice(input_real, first_group, groups_here)
    local_in_imag = local_slice(input_imag, first_group, groups_here)
    drive_real = factor_real[..., None] * local_in_real - factor_imag[..., None] * local_in_imag
    drive_imag = factor_real[..., None] * local_in_imag + factor_imag[..., None] * local_in_real
    drive_matrix_real = jnp.einsum("gnc,gh->gchn", drive_real, group_identity).reshape(
        state_width, state_columns
    )
    drive_matrix_imag = jnp.einsum("gnc,gh->gchn", drive_imag, group_identity).reshape(
        state_width, state_columns
    )
    signal = state_in.astype(jnp.float32)
    push_real = jnp.dot(signal, drive_matrix_real, precision=highest)
    push_imag = jnp.dot(signal, drive_matrix_imag, precision=highest)
    decay_wide_real = jnp.broadcast_to(decay_real, push_real.shape)
    decay_wide_imag = jnp.broadcast_to(decay_imag, push_real.shape)
    _, _, local_real, local_imag = lax.associative_scan(
        scan_combine, (decay_wide_real, decay_wide_imag, push_real, push_imag), axis=0
    )
    end_state = jnp.stack([local_real[row_count - 1], local_imag[row_count - 1]])
    block_magnitude = jnp.exp(row_count * exponent)
    block_decay = jnp.stack(
        [block_magnitude * jnp.cos(row_count * angle), block_magnitude * jnp.sin(row_count * angle)]
    )
    last_rows = pool_in[row_count - window_reach :]
    identity = (
        jnp.stack([jnp.ones_like(exponent), jnp.zeros_like(exponent)]),
        jnp.zeros_like(end_state),
    )
    _, incoming = entering((block_decay, end_state), "sp", chain_combine, identity)
    halo_block = passed_along(last_rows, "sp", 1)
    positions = (jnp.arange(row_count, dtype=jnp.float32) + 1.0)[:, None]
    power_magnitude = jnp.exp(positions * exponent[None, :])
    power_angle = positions * angle[None, :]
    power_cos = power_magnitude * jnp.cos(power_angle)
    power_sin = power_magnitude * jnp.sin(power_angle)
    states_real = local_real + power_cos * incoming[0] - power_sin * incoming[1]
    states_imag = local_imag + power_cos * incoming[1] + power_sin * incoming[0]
    local_out_real = local_slice(output_real, first_group, groups_here)
    local_out_imag = local_slice(output_imag, first_group, groups_here)
    read_matrix_real = jnp.einsum("gcn,gh->hngc", local_out_real, group_identity).reshape(
        state_columns, state_width
    )
    read_matrix_imag = jnp.einsum("gcn,gh->hngc", local_out_imag, group_identity).reshape(
        state_columns, state_width
    )
    readout_sum = jnp.dot(states_real, read_matrix_real, precision=highest)
    readout_sum = readout_sum - jnp.dot(states_imag, read_matrix_imag, precision=highest)
    readout_sum = (
        readout_sum + local_slice(skip_gain, head_index * state_width, state_width) * signal
    )
    state_out = jax.nn.gelu(readout_sum).astype(jnp.bfloat16)
    pool_groups_here = pool_width // POOL_GROUP
    first_pool = head_index * pool_groups_here
    extended = jnp.concatenate([halo_block, pool_in], axis=0)
    column_group = first_pool + jnp.arange(pool_width, dtype=jnp.int32) // POOL_GROUP
    column_window = jnp.left_shift(jnp.ones_like(column_group), column_group % 4 + 1)
    targets = jnp.arange(row_count, dtype=jnp.int32)[:, None] + window_reach
    sources = jnp.arange(row_count + window_reach, dtype=jnp.int32)[None, :]
    window_sums = jnp.zeros((row_count, pool_width), jnp.float32)
    for power_index in range(1, 5):
        span_width = 2**power_index
        band_mask = ((sources <= targets) & (sources > targets - span_width)).astype(jnp.bfloat16)
        partial_sums = jnp.dot(band_mask, extended, preferred_element_type=jnp.float32)
        window_sums = jnp.where(column_window[None, :] == span_width, partial_sums, window_sums)
    global_rows = block_index * row_count + jnp.arange(row_count, dtype=jnp.int32)
    divisor = jnp.minimum(global_rows[:, None] + 1, column_window[None, :]).astype(jnp.float32)
    pooled = window_sums / divisor - pool_in.astype(jnp.float32)
    pool_identity = jnp.eye(pool_groups_here, dtype=jnp.float32)
    mixer_matrix = jnp.einsum(
        "gcd,gh->gchd",
        local_slice(pool_weight, first_pool, pool_groups_here).astype(jnp.float32),
        pool_identity,
    ).reshape(pool_width, pool_width)
    projected = jnp.dot(pooled, mixer_matrix, precision=highest)
    pool_out = (projected * local_slice(pool_gain, head_index * pool_width, pool_width)).astype(
        jnp.bfloat16
    )
    pieces = in_one_piece((state_out, pool_out), TP, 1, 0)
    state_rows = state_out_full
    pool_rows = pool_out_full
    running_sum = jnp.dot(pieces[0], state_rows, preferred_element_type=jnp.float32)
    combined = running_sum + jnp.dot(pieces[1], pool_rows, preferred_element_type=jnp.float32)
    return combined.astype(jnp.bfloat16)


def solution(mesh):
    finer = Mesh(mesh.devices.reshape(mesh.shape["sp"], 4, 2), ("sp", "tp_0", "tp_1"))
    in_specs = (
        P("sp", TP),
        P(),
        P("sp", TP),
        P("sp", TP),
        P(),
        P(),
        P(),
        P(),
        P(),
        P(),
        P(),
        P(),
        P(),
        P(),
        P("sp", TP),
        P("sp", TP),
    )
    out_specs = P("sp", TP)
    return jax.shard_map(body, mesh=finer, in_specs=in_specs, out_specs=out_specs, check_vma=False)
```

profile of v0, /device:TPU:1, one launch (start us, length us, event | category | flops | bytes accessed | tf_op | source)
XLA Modules:
  0.0 148.7 jit_solution(3745280262288060132)
XLA Ops:
  6.5 1.5 pad_maximum_fusion.6
  8.1 1.5 pad_maximum_fusion.7
  9.6 1.0 fusion.82
  10.6 12.1 %all-gather = bf16[512,384]{1,0:T(8,128)(2,1)S(1)} all-gather(bf16[128,384]{1,0:T(8,128)(2,1)S(1)} %get-tuple-element.34), channel_id=2, replica_groups=mesh['sp'=16,'tp_0'=4,'tp_1'=2] {'tp_0'}, dimensions={0}, use_global_device_ids=true | all-gather | bytes 491520 | tf_op jit(solution)/shard_map/all_gather | solution.py:34
  22.7 4.4 %all_gather.22 = bf16[8,128,384]{2,1,0:T(8,128)(2,1)S(1)} all-gather(bf16[4,128,384]{2,1,0:T(8,128)(2,1)S(1)} %bitcast.101), channel_id=1, replica_groups=mesh['sp'=16,'tp_0'=4,'tp_1'=2] {'tp_1'}, dimensions={0}, use_global_device_ids=true | all-gather | bytes 1179648 | tf_op jit(solution)/shard_map/all_gather | solution.py:34
  27.2 2.0 %all-gather.1 = bf16[256,384]{1,0:T(8,128)(2,1)S(1)} all-gather(bf16[128,384]{1,0:T(8,128)(2,1)S(1)} %get-tuple-element.35), channel_id=3, replica_groups=mesh['sp'=16,'tp_0'=4,'tp_1'=2] {'tp_1'}, dimensions={0}, use_global_device_ids=true | all-gather | bytes 294912 | tf_op jit(solution)/shard_map/all_gather | solution.py:34
  29.1 12.3 %all_gather.24 = bf16[8,128,384]{2,1,0:T(8,128)(2,1)S(1)} all-gather(bf16[2,128,384]{2,1,0:T(8,128)(2,1)S(1)} %bitcast.102), channel_id=1, replica_groups=mesh['sp'=16,'tp_0'=4,'tp_1'=2] {'tp_0'}, dimensions={0}, use_global_device_ids=true | all-gather | bytes 983040 | tf_op jit(solution)/shard_map/all_gather | solution.py:34
  42.4 0.8 cosine_multiply_fusion
  43.9 0.8 multiply_subtract_fusion.1
  50.5 0.9 multiply_add_fusion
  51.4 1.2 multiply_bitcast_fusion.2
  52.6 1.2 reshape.823
  53.9 2.3 %copy.76 = f32[256,8,384]{0,2,1:T(8,128)} copy(f32[256,8,384]{2,0,1:T(8,128)S(1)} %convert_bitcast_fusion) | data formatting | bytes 6291456 | tf_op jit(solution)/shard_map/convert_element_type | solution.py:179
  56.8 1.9 %reshape.826 = f32[128,512]{1,0:T(8,128)} reshape(f32[8,16,8,64]{3,2,1,0:T(8,128)} %get-tuple-element.105) | data formatting | bytes 524288 | tf_op jit(solution)/shard_map/reshape | solution.py:214
  60.9 0.9 constant_dynamic-slice_fusion
  61.8 1.2 multiply_bitcast_fusion
  63.0 2.0 %reshape.827 = f32[512,128]{0,1:T(8,128)} reshape(f32[8,64,8,16]{1,0,3,2:T(8,128)} %get-tuple-element.100) | data formatting | bytes 524288 | tf_op jit(solution)/shard_map/reshape | solution.py:246
  65.0 1.9 %reshape.828 = f32[512,128]{0,1:T(8,128)} reshape(f32[8,64,8,16]{1,0,3,2:T(8,128)} %get-tuple-element.99) | data formatting | bytes 524288 | tf_op jit(solution)/shard_map/reshape | solution.py:249
  69.8 1.3 dynamic_slice.37
  71.1 1.3 dynamic_slice.39
  72.5 2.3 %fusion.1 = bf16[256,3072]{0,1:T(8,128)(2,1)} fusion(f32[256,8,384]{0,2,1:T(8,128)S(1)} %copy-done, f32[3072]{0:T(1024)} %param.17), kind=kLoop, calls=%fused_computation.4 | loop fusion | flops 1572864 | bytes 4730880 | tf_op jit(solution)/shard_map/convert_element_type | solution.py:180
  74.9 2.2 %fusion.6 = bf16[256,128]{1,0:T(8,128)(2,1)S(1)} fusion(bf16[256,3072]{0,1:T(8,128)(2,1)} %fusion.1, bf16[3072,256]{1,0:T(8,128)(2,1)} %all-gather.6.cloned.1.call-done, f32[256]{0:T(256)S(1)} %copy-done.14), kind=kOutput, calls=%fused_computation.19 | convolution fusion | flops 201392128 | bytes 2425856 | tf_op jit(solution)/shard_map/dot_general | solution.py:183
  83.8 1.7 %pad.126 = f32[256,512]{1,0:T(8,128)} pad(f32[128,512]{1,0:T(8,128)S(1)} %pad_maximum_fusion.1, f32[]{:T(128)} %constant.43.clone.1), padding=0_1_1x0_0_0 | pad | bytes 786436 | tf_op jit(solution)/shard_map/pad | solution.py:222
  85.8 1.8 %fusion.7 = bf16[256,128]{1,0:T(8,128)(2,1)S(1)} fusion(bf16[256,3072]{0,1:T(8,128)(2,1)S(1)} %copy-done.3, bf16[3072,256]{1,0:T(8,128)(2,1)} %all-gather.6.cloned.1.call-done, f32[256]{0:T(256)S(1)} %copy-done.15), kind=kOutput, calls=%fused_computation.20 | convolution fusion | flops 201392128 | bytes 2425856 | tf_op jit(solution)/shard_map/dot_general | solution.py:184
  87.6 3.3 %collective-permute-start = (bf16[16,128]{1,0:T(8,128)(2,1)S(1)}, bf16[16,128]{1,0:T(8,128)(2,1)S(1)}, u32[]{:S(2)}, u32[]{:S(2)}) collective-permute-start(bf16[16,128]{1,0:T(8,128)(2,1)S(1)} %slice.724), channel_id=1, source_target_pairs={{0,8},{8,16},{16,24},{24,32},{32,40},{40,48},{48,56},{56,64},{64,7... | collective-permute-start | bytes 12296 | tf_op jit(solution)/shard_map/ppermute | solution.py:108
  92.4 7.3 %all-to-all-start = ((f32[16,4,512]{2,1,0:T(4,128)}), f32[16,4,512]{2,1,0:T(4,128)S(1)}, u32[]{:S(2)}, u32[]{:S(2)}) async-start(f32[16,4,512]{2,1,0:T(4,128)} %broadcast_in_dim.80), calls=%async_computation | async-start | bytes 262144 | tf_op jit(solution)/shard_map/all_to_all | solution.py:61
  101.4 5.0 %all-to-all-done = f32[16,4,512]{2,1,0:T(4,128)S(1)} async-done(((f32[16,4,512]{2,1,0:T(4,128)}), f32[16,4,512]{2,1,0:T(4,128)S(1)}, u32[]{:S(2)}, u32[]{:S(2)}) %all-to-all-start) | async-done | bytes 131104 | tf_op jit(solution)/shard_map/all_to_all | solution.py:61
  107.2 2.6 %fusion.26 = f32[256,128]{1,0:T(8,128)S(1)} fusion(f32[512,128]{0,1:T(8,128)S(1)} %copy-done.7, f32[256,512]{1,0:T(8,128)S(1)} %copy-done.5, f32[256,512]{1,0:T(8,128)S(1)} %pad.127, f32[512]{0:T(512)S(1)} %bitcast.105, f32[512]{0:T(512)S(1)} %bitcast.103, f32[512]{0:T(512)S(1)} %copy-done.13, f32[512]{0:T(512)S(1)} %copy-done.12, f32[256]{0:T(256)S(1)} %copy-done.25), kind=kOutput, calls=%fused_computation.45 | convolution fusion | flops 202506240 | bytes 1451008 | tf_op jit(solution)/shard_map/dot_general | solution.py:252
  109.9 2.6 %fusion.67 = bf16[256,128]{1,0:T(8,128)(2,1)S(1)} fusion(f32[256,128]{1,0:T(8,128)S(1)} %fusion.26, f32[512,128]{0,1:T(8,128)S(1)} %copy-done.6, f32[256,512]{1,0:T(8,128)S(1)} %pad.128, f32[256,512]{1,0:T(8,128)S(1)} %pad.129, f32[512]{0:T(512)S(1)} %bitcast.106, f32[512]{0:T(512)S(1)} %bitcast.104, f32[512]{0:T(512)S(1)} %copy-done.13, ...), kind=kOutput, calls=%fused_computation.91 | convolution fusion | flops 202932224 | bytes 1582592 | tf_op jit(solution)/shard_map/dot_general | solution.py:253
  113.3 25.0 %all-gather.8.cloned.1.call-done = bf16[512,1024]{1,0:T(8,128)(2,1)} async-done(((bf16[512,128]{1,0:T(8,128)(2,1)}), bf16[512,1024]{1,0:T(8,128)(2,1)}) %all-gather.8.cloned.1.call-update) | async-done | bytes 1048592 | tf_op jit(solution)/shard_map/all_gather | solution.py:20
  138.2 1.7 %fusion.10 = f32[256,384]{1,0:T(8,128)S(1)} fusion(bf16[1024,768]{1,0:T(8,128)(2,1)} %all-gather.10.cloned.1.call-done, bf16[512,1024]{1,0:T(8,128)(2,1)} %all-gather.8.cloned.1.call-done), kind=kOutput, calls=%fused_computation.23 | convolution fusion | flops 201326592 | bytes 1703936 | tf_op jit(solution)/shard_map/dot_general | solution.py:287
  140.0 2.2 %fusion.2 = bf16[256,384]{1,0:T(8,128)(2,1)} fusion(f32[256,384]{1,0:T(8,128)S(1)} %fusion.10, bf16[1024,768]{1,0:T(8,128)(2,1)S(1)} %copy-done.20, bf16[512,1024]{1,0:T(8,128)(2,1)} %all-gather.8.cloned.1.call-done), kind=kOutput, calls=%fused_computation.7 | convolution fusion | flops 201523200 | bytes 1900544 | tf_op jit(solution)/shard_map/dot_general | solution.py:288
  (265 shorter events, 23.9 us)
Async XLA Ops:
  6.5 68.3 %all-gather.6.cloned.1.call-start = ((), (), s32[]{:S(2)}) async-start(), calls=%async_computation.1 | async-start | bytes 1671168 | tf_op jit(solution)/shard_map/all_gather | solution.py:20
  8.0 105.2 %all-gather.10.cloned.1.call-start = ((), (), s32[]{:S(2)}) async-start(), calls=%async_computation.3 | async-start | bytes 1671168 | tf_op jit(solution)/shard_map/all_gather | solution.py:20
  61.8 10.7 %copy-start = (f32[256,8,384]{0,2,1:T(8,128)S(1)}, f32[256,8,384]{0,2,1:T(8,128)}, u32[]{:S(2)}) copy-start(f32[256,8,384]{0,2,1:T(8,128)} %copy.76) | copy-start | bytes 9437188
  77.5 4.4 %copy-start.1 = (f32[256,512]{1,0:T(8,128)}, f32[256,512]{1,0:T(8,128)S(1)}, u32[]{:S(2)}) copy-start(f32[256,512]{1,0:T(8,128)S(1)} %fusion.90) | copy-start | bytes 1572868
  78.6 3.3 %copy-start.2 = (f32[256,512]{1,0:T(8,128)}, f32[256,512]{1,0:T(8,128)S(1)}, u32[]{:S(2)}) copy-start(f32[256,512]{1,0:T(8,128)S(1)} %fusion.91) | copy-start | bytes 1572868
  85.6 6.0 %copy-start.9 = (f32[1,512]{1,0:T(1,128)S(1)}, f32[1,512]{1,0:T(1,128)}, u32[]{:S(2)}) copy-start(f32[1,512]{1,0:T(1,128)} %mul.1291) | copy-start | bytes 6148
  85.6 6.0 %copy-start.10 = (f32[1,512]{1,0:T(1,128)S(1)}, f32[1,512]{1,0:T(1,128)}, u32[]{:S(2)}) copy-start(f32[1,512]{1,0:T(1,128)} %mul.1289) | copy-start | bytes 6148
  85.7 14.1 %copy-start.17 = (s32[256]{0:T(256)S(1)}, s32[256]{0:T(256)}, u32[]{:S(2)}) copy-start(s32[256]{0:T(256)} %get-tuple-element.116) | copy-start | bytes 3076
  85.7 14.1 %copy-start.24 = (pred[128]{0:T(512)(128)(4,1)S(1)}, pred[128]{0:T(512)(128)(4,1)}, u32[]{:S(2)}) copy-start(pred[128]{0:T(512)(128)(4,1)} %get-tuple-element.107) | copy-start | bytes 388
  85.7 14.1 %copy-start.27 = (s32[256]{0:T(256)S(1)}, s32[256]{0:T(256)}, u32[]{:S(2)}) copy-start(s32[256]{0:T(256)} %iota_add_fusion) | copy-start | bytes 3076
  85.7 14.4 %copy-start.28 = (s32[256]{0:T(256)S(1)}, s32[256]{0:T(256)}, u32[]{:S(2)}) copy-start(s32[256]{0:T(256)} %iota_add_fusion.1) | copy-start | bytes 3076
  85.8 14.4 %copy-start.31 = (pred[128]{0:T(512)(128)(4,1)S(1)}, pred[128]{0:T(512)(128)(4,1)}, u32[]{:S(2)}) copy-start(pred[128]{0:T(512)(128)(4,1)} %broadcast_compare_fusion.3) | copy-start | bytes 388
  85.8 14.7 %copy-start.23 = (pred[128]{0:T(512)(128)(4,1)S(1)}, pred[128]{0:T(512)(128)(4,1)}, u32[]{:S(2)}) copy-start(pred[128]{0:T(512)(128)(4,1)} %get-tuple-element.108) | copy-start | bytes 388
  85.8 14.7 %copy-start.26 = (s32[256]{0:T(256)S(1)}, s32[256]{0:T(256)}, u32[]{:S(2)}) copy-start(s32[256]{0:T(256)} %iota_add_fusion.2) | copy-start | bytes 3076
  87.5 13.3 %copy-start.16 = (s32[256]{0:T(256)S(1)}, s32[256]{0:T(256)}, u32[]{:S(2)}) copy-start(s32[256]{0:T(256)} %get-tuple-element.115) | copy-start | bytes 3076
  87.6 13.3 %copy-start.29 = (pred[128]{0:T(512)(128)(4,1)S(1)}, pred[128]{0:T(512)(128)(4,1)}, u32[]{:S(2)}) copy-start(pred[128]{0:T(512)(128)(4,1)} %broadcast_compare_fusion.2) | copy-start | bytes 388
  87.6 13.3 %copy-start.30 = (s32[128]{0:T(128)S(1)}, s32[128]{0:T(128)}, u32[]{:S(2)}) copy-start(s32[128]{0:T(128)} %fusion.76) | copy-start | bytes 1540
  87.6 13.6 %copy-start.8 = (f32[128,128]{1,0:T(8,128)S(1)}, f32[128,128]{1,0:T(8,128)}, u32[]{:S(2)}) copy-start(f32[128,128]{1,0:T(8,128)} %reshape.829) | copy-start | bytes 196612
  87.6 13.6 %copy-start.19 = (f32[128]{0:T(128)S(1)}, f32[128]{0:T(128)}, u32[]{:S(2)}) copy-start(f32[128]{0:T(128)} %dynamic_slice.39) | copy-start | bytes 1540
  87.6 12.2 %collective-permute-start = (bf16[16,128]{1,0:T(8,128)(2,1)S(1)}, bf16[16,128]{1,0:T(8,128)(2,1)S(1)}, u32[]{:S(2)}, u32[]{:S(2)}) collective-permute-start(bf16[16,128]{1,0:T(8,128)(2,1)S(1)} %slice.724), channel_id=1, source_target_pairs={{0,8},{8,16},{16,24},{24,32},{32,40},{40,48},{48,56},{56,64},{64,7... | collective-permute-start | bytes 12296 | tf_op jit(solution)/shard_map/ppermute | solution.py:108
  92.4 14.1 %copy-start.11 = (f32[2,512]{1,0:T(2,128)S(1)}, f32[2,512]{1,0:T(2,128)}, u32[]{:S(2)}) copy-start(f32[2,512]{1,0:T(2,128)} %constant.100.clone.1) | copy-start | bytes 12292
  92.4 14.1 %copy-start.18 = (pred[16]{0:T(512)(128)(4,1)S(1)}, pred[16]{0:T(512)(128)(4,1)}, u32[]{:S(2)}) copy-start(pred[16]{0:T(512)(128)(4,1)} %iota_compare_fusion.7) | copy-start | bytes 52
  92.4 14.1 %all-to-all-start = ((f32[16,4,512]{2,1,0:T(4,128)}), f32[16,4,512]{2,1,0:T(4,128)S(1)}, u32[]{:S(2)}, u32[]{:S(2)}) async-start(f32[16,4,512]{2,1,0:T(4,128)} %broadcast_in_dim.80), calls=%async_computation | async-start | bytes 262144 | tf_op jit(solution)/shard_map/all_to_all | solution.py:61
  99.6 38.6 %all-gather.8.cloned.1.call-start = ((), (), s32[]{:S(2)}) async-start(), calls=%async_computation.2 | async-start | bytes 1179648 | tf_op jit(solution)/shard_map/all_gather | solution.py:20
  100.5 6.7 %copy-start.5 = (f32[256,512]{1,0:T(8,128)S(1)}, f32[256,512]{1,0:T(8,128)}, u32[]{:S(2)}) copy-start(f32[256,512]{1,0:T(8,128)} %pad.126) | copy-start | bytes 1572868
  100.5 6.7 %copy-start.7 = (f32[512,128]{0,1:T(8,128)S(1)}, f32[512,128]{0,1:T(8,128)}, u32[]{:S(2)}) copy-start(f32[512,128]{0,1:T(8,128)} %reshape.827) | copy-start | bytes 786436
  100.5 6.7 %copy-start.12 = (f32[512]{0:T(512)S(1)}, f32[512]{0:T(512)}, u32[]{:S(2)}) copy-start(f32[512]{0:T(512)} %mul.1279) | copy-start | bytes 6148
  100.5 6.7 %copy-start.13 = (f32[512]{0:T(512)S(1)}, f32[512]{0:T(512)}, u32[]{:S(2)}) copy-start(f32[512]{0:T(512)} %mul.1282) | copy-start | bytes 6148
  100.5 6.7 %copy-start.25 = (f32[256]{0:T(256)S(1)}, f32[256]{0:T(256)}, u32[]{:S(2)}) copy-start(f32[256]{0:T(256)} %iota_add_fusion.4) | copy-start | bytes 3076
  101.4 8.5 %copy-start.6 = (f32[512,128]{0,1:T(8,128)S(1)}, f32[512,128]{0,1:T(8,128)}, u32[]{:S(2)}) copy-start(f32[512,128]{0,1:T(8,128)} %reshape.828) | copy-start | bytes 786436
  101.4 8.5 %copy-start.22 = (f32[128]{0:T(128)S(1)}, f32[128]{0:T(128)}, u32[]{:S(2)}) copy-start(f32[128]{0:T(128)} %dynamic_slice.37) | copy-start | bytes 1540
  113.3 26.7 %copy-start.20 = (bf16[1024,768]{1,0:T(8,128)(2,1)S(1)}, bf16[1024,768]{1,0:T(8,128)(2,1)}, u32[]{:S(2)}) copy-start(bf16[1024,768]{1,0:T(8,128)(2,1)} %all-gather.10.cloned.1.call-done) | copy-start | bytes 4718596
  (7 other events, 10.9 us)
Sparse Core Ops, SparseCore 0:
  9.5 45.7 all-gather.5
  57.4 43.1 all-gather.9
  113.3 24.8 all-gather.7
where the time goes:
time: 150 us; the launch traced here: 149 us
  blocking collectives  30.8 us (21%)
  waiting for transfers between devices  30.1 us (20%)
  local copies, waits for them, and re-layouts  25 us (17%)
  other arithmetic  22.2 us (15%)
  matrix products  15.2 us (10%)
  between operations  14.6 us (10%)
  starting transfers between devices  10.8 us (7%)
    all_gather x4, blocking collectives, stacked_from(): parts = lax.all_gather(parts, axes[k], axis=0, tiled=True)  30.8 us
    all_gather x3, waiting for transfers between devices, in_one_piece(): result = lax.all_gather(both, axis, axis=dim, tiled=True)  25 us
    all_to_all x1, starting transfers between devices, copy_for_each(): lax.all_to_all(jnp.broadcast_to(array[None], (peers, *array.shape)), axis...  7.26 us
    all_to_all x1, waiting for transfers between devices, copy_for_each(): lax.all_to_all(jnp.broadcast_to(array[None], (peers, *array.shape)), axis...  5.02 us
    slice x54, local copies, waits for them, and re-layouts, body(): lax.associative_scan(scan_combine, (decay_wide_real, decay_wide_imag, pus...  3.79 us
    concatenate x3, other arithmetic, in_one_piece(): both = jnp.concatenate(arrays, axis=along)  3.61 us
    dynamic_slice x3, local copies, waits for them, and re-layouts, local_slice(): return lax.dynamic_slice_in_dim(array, first_index, count_here, 0)  3.52 us
    ppermute x1, starting transfers between devices, passed_along(): lax.ppermute(value, axis, [(source, source + steps) for source in range(f...  3.29 us
  transfers between devices with their start and end apart: 5, of which 2 were waited for; matrix products, arithmetic and copies ran while one was open for 38% of the time, Pallas kernels for 0%

commit v1 on v0

v1 whole, which is shorter than its diff:
```python
import functools

import jax
import jax.numpy as jnp
from jax import lax
from jax.experimental import pallas as pl
from jax.experimental.pallas import tpu as pltpu
from jax.sharding import PartitionSpec as P

EPSILON = 1e-06
HIGHEST = lax.Precision.HIGHEST
MESH = pl.DeviceIdType.MESH
F32, BF16 = jnp.float32, jnp.bfloat16

ROWS = 256
STEPS, PARTS = 32, 8
FEATURES = 384
PEERS, HEADS_TP = 16, 8
GROUPS, STATE, CHANNEL = 8, 64, 16
WIDTH = GROUPS * STATE
REACH = 16


def iota(shape, dim):
    return lax.broadcasted_iota(jnp.int32, shape, dim)


def position_of(row):
    return STEPS * (row % PARTS) + row // PARTS


def dot(a, b, precision=None):
    return jnp.dot(a, b, preferred_element_type=F32, precision=precision)


def split(value):
    high = value.astype(BF16)
    return high, (value - high.astype(F32)).astype(BF16)


class Move:
    def __init__(self, sends, fills, device, sems, index):
        self.sends, self.fills, self.device, self.sems, self.index = sends, fills, device, sems, index

    def _copy(self, ref):
        return pltpu.make_async_remote_copy(
            src_ref=ref, dst_ref=ref, send_sem=self.sems[0].at[self.index], recv_sem=self.sems[1].at[self.index],
            device_id=self.device, device_id_type=MESH)

    def start(self):
        self._copy(self.sends).start()

    def arrive(self):
        self._copy(self.fills).wait_recv()

    def left(self):
        self._copy(self.sends).wait_send()


class LineGather:
    def __init__(self, slot, sems, first, y, c):
        d = 1 - 2 * c
        at = lambda k, core: slot(lax.rem(y + k + 4, 4) * 2 + core)
        to = lambda k, core: {"tp": lax.rem(y + k + 4, 4) * 2 + core}
        o = 1 - c
        mk = lambda s, f, dev, i: Move(s, f, dev, sems, first + i)
        self.ahead = mk(at(0, c), at(-d, c), to(d, c), 0)
        self.back = mk(at(0, c), at(d, c), to(-d, c), 1)
        self.onward = mk(at(-d, c), at(-2 * d, c), to(d, c), 2)
        self.own = mk(at(0, c), at(0, o), to(0, o), 3)
        self.cross_ahead = mk(at(-d, c), at(d, o), to(0, o), 4)
        self.cross_back = mk(at(d, c), at(-d, o), to(0, o), 5)
        self.cross_far = mk(at(-2 * d, c), at(2 * d, o), to(0, o), 6)
        self.all = [self.ahead, self.back, self.onward, self.own, self.cross_ahead, self.cross_back, self.cross_far]
        index = lambda k, core: lax.rem(y + k + 4, 4) * 2 + core
        self.index = dict(own=index(0, c), ahead=index(-d, c), back=index(d, c), onward=index(-2 * d, c),
                          p_own=index(0, o), p_ahead=index(d, o), p_back=index(-d, o), p_onward=index(2 * d, o))


class PlaneGather:
    def __init__(self, slot_a, slot_b, sems, first, z, x):
        wrap = lambda k: lax.rem(k + 4, 4)
        at = lambda dz, dx: wrap(z + dz) * 4 + wrap(x + dx)
        self.count = 0

        def mk(slot, sent, filled, device):
            move = Move(slot(at(*sent)), slot(at(*filled)), {"sp": at(*device)}, sems, first + self.count)
            self.count += 1
            return move

        def ring(slot, along, e, base):
            v = (lambda k: (base, k)) if along == "x" else (lambda k: (k, base))
            w = (lambda k: (0, k)) if along == "x" else (lambda k: (k, 0))
            return [
                mk(slot, v(0), v(-e), w(e)),
                mk(slot, v(0), v(e), w(-e)),
                mk(slot, v(-e), v(-2 * e), w(e)),
            ]

        self.a = ring(slot_a, "x", 1, 0)
        self.b = ring(slot_b, "z", -1, 0)
        heavy = {0: 1, -1: 1, 1: -1, 2: -1}
        self.za = {o: ring(slot_a, "z", heavy[o], o) for o in (0, -1, 1, 2)}
        self.xb = {o: ring(slot_b, "x", -heavy[o], o) for o in (0, -1, 1, 2)}
        self.all = [*self.a, *self.b, *(m for r in self.za.values() for m in r), *(m for r in self.xb.values() for m in r)]

    def begin(self):
        for m in (self.a[0], self.a[1], self.b[0], self.b[1], self.za[0][0], self.za[0][1], self.xb[0][0], self.xb[0][1]):
            m.start()

    def events(self):
        def first_of(move, more, ring):
            def event():
                move.arrive()
                if more is not None:
                    more.start()
                ring[0].start()
                ring[1].start()
            return event

        def onward(ring):
            def event():
                ring[0].arrive()
                ring[2].start()
            return event

        def rest():
            for rings in (self.za, self.xb):
                for o in (0, -1, 1, 2):
                    rings[o][1].arrive()
                    rings[o][2].arrive()

        return [
            first_of(self.a[0], self.a[2], self.za[-1]), first_of(self.b[0], self.b[2], self.xb[1]),
            first_of(self.a[1], None, self.za[1]), first_of(self.b[1], None, self.xb[-1]),
            onward(self.za[0]), onward(self.xb[0]),
            first_of(self.a[2], None, self.za[2]), first_of(self.b[2], None, self.xb[2]),
            onward(self.za[-1]), onward(self.xb[1]), onward(self.za[1]), onward(self.xb[-1]),
            onward(self.za[2]), onward(self.xb[2]), rest,
        ]


def kernel(
    tokens, gain_all, state_in_w, pool_in_w, rate_real_all, rate_imag_all, log_step_all, input_real, input_imag,
    output_real, output_imag, skip_all, pool_weight, pool_gain_all, state_out_w, pool_out_w, out,
    gain, rate_real, rate_imag, log_step, skip_gain, pool_gain, own_tokens, tok, scaled, win, wst, wpo, in_re, in_im, out_re, out_im, mix_raw,
    drive, read, unsort, bands, tails, recip, push, high, low, ends, halo, sbuf, pbuf,
    local_sem, tok_send, tok_recv, win_send, win_recv, wout_send, wout_recv,
    end_send, end_recv, halo_send, halo_recv, s_send, s_recv, p_send, p_recv,
):
    s, t = lax.axis_index("sp"), lax.axis_index("tp")
    z, x, y, c = s // 4, s % 4, t // 2, t % 2
    g0 = t * GROUPS

    def lanes(ref, index, width):
        return ref.at[:, pl.ds(pl.multiple_of(index * width, 128), width)]

    def rows(ref, start, count):
        return ref.at[pl.ds(pl.multiple_of(start, 16), count), :]

    loads = [
        (tokens, own_tokens),
        (state_in_w, win.at[pl.ds(pl.multiple_of(s * 192, 16), 192), 0:128]),
        (pool_in_w, win.at[pl.ds(pl.multiple_of(s * 192, 16), 192), 128:256]),
        (state_out_w, rows(wst, s * 64, 64)),
        (pool_out_w, rows(wpo, s * 64, 64)),
        (input_real.at[pl.ds(g0, GROUPS)], in_re),
        (input_imag.at[pl.ds(g0, GROUPS)], in_im),
        (output_real.at[pl.ds(g0, GROUPS)], out_re),
        (output_imag.at[pl.ds(g0, GROUPS)], out_im),
        (pool_weight.at[pl.ds(2 * t, 2)], mix_raw),
        (gain_all, gain),
        (rate_real_all.at[pl.ds(pl.multiple_of(g0, 8), GROUPS), :], rate_real),
        (rate_imag_all.at[pl.ds(pl.multiple_of(g0, 8), GROUPS), :], rate_imag),
        (log_step_all, log_step),
        (lanes(skip_all, t, 128), skip_gain),
        (lanes(pool_gain_all, t, 128), pool_gain),
    ]
    loads = [pltpu.make_async_copy(a, b, local_sem.at[k]) for k, (a, b) in enumerate(loads)]
    for load in loads:
        load.start()

    barrier = pltpu.get_barrier_semaphore()
    for k in range(1, PEERS):
        pl.semaphore_signal(barrier, inc=1, device_id={"sp": lax.rem(s + k, PEERS)}, device_id_type=MESH)
    for k in range(1, HEADS_TP):
        pl.semaphore_signal(barrier, inc=1, device_id={"tp": lax.rem(t + k, HEADS_TP)}, device_id_type=MESH)

    r0, r1 = iota((ROWS, ROWS), 0), iota((ROWS, ROWS), 1)
    loads[0].wait()
    sort = (position_of(r0) == r1).astype(BF16)
    lanes(tok, t, FEATURES)[...] = dot(sort, own_tokens[...]).astype(BF16)
    unsort[...] = (position_of(r1) == r0).astype(BF16)

    line = LineGather(lambda p: lanes(tok, p, FEATURES), (tok_send, tok_recv), 0, y, c)
    w_in = PlaneGather(
        lambda q: rows(win, q * 192, 96), lambda q: rows(win, q * 192 + 96, 96), (win_send, win_recv), 0, z, x)
    w_out = PlaneGather(
        lambda q: rows(wst, q * 64, 64), lambda q: rows(wpo, q * 64, 64), (wout_send, wout_recv), 0, z, x)
    for load in loads[1:]:
        load.wait()

    pl.semaphore_wait(barrier, PEERS - 1 + HEADS_TP - 1)
    line.ahead.start()
    line.back.start()
    line.own.start()
    w_in.begin()

    wanted = iota((GROUPS, STATE), 0) + g0
    steps_log = jnp.sum(jnp.where(iota((GROUPS, 64), 1) == wanted, log_step[...], 0.0), axis=1, keepdims=True)
    step = jnp.exp(steps_log) / float(ROWS * PEERS)
    real = rate_real[...]
    imag = rate_imag[...]
    exponent, angle = real * step, imag * step
    magnitude = jnp.exp(exponent)
    cosine, sine, half_sine = jnp.cos(angle), jnp.sin(angle), jnp.sin(0.5 * angle)
    decay_real, decay_imag = magnitude * cosine, magnitude * sine
    less = exponent * (1.0 + exponent * 0.5 * (1.0 + exponent * (1.0 / 3.0) * (1.0 + exponent * 0.25)))
    less = less * cosine - 2.0 * half_sine * half_sine
    denominator = real * real + imag * imag
    factor_real = (less * real + decay_imag * imag) / denominator
    factor_imag = (decay_imag * real - less * imag) / denominator

    spread = (iota((STATE, WIDTH), 1) % STATE == iota((STATE, WIDTH), 0)).astype(F32)
    own_group = iota((GROUPS, WIDTH), 1) // STATE == iota((GROUPS, WIDTH), 0)

    def flat(value):
        return jnp.sum(jnp.where(own_group, dot(value, spread, HIGHEST), 0.0), axis=0, keepdims=True)

    lr, li = flat(decay_real), flat(decay_imag)
    fr, fi = flat(factor_real), flat(factor_imag)

    def times(ar, ai, br, bi):
        return ar * br - ai * bi, ar * bi + ai * br

    pr, pi = lr, li
    for _ in range(5):
        pr, pi = times(pr, pi, pr, pi)
    part_real, part_imag = pr, pi
    for _ in range(3):
        pr, pi = times(pr, pi, pr, pi)
    block_real, block_imag = pr, pi
    sub = iota((PARTS, WIDTH), 0)
    up_real, up_imag = jnp.ones((PARTS, WIDTH), F32), jnp.zeros((PARTS, WIDTH), F32)
    down_real, down_imag = up_real, up_imag
    wr, wi = jnp.ones((1, WIDTH), F32), jnp.zeros((1, WIDTH), F32)
    for k in range(1, PARTS):
        wr, wi = times(wr, wi, part_real, part_imag)
        up_real, up_imag = jnp.where(sub == k, wr, up_real), jnp.where(sub == k, wi, up_imag)
        down_real = jnp.where(sub == PARTS - 1 - k, wr, down_real)
        down_imag = jnp.where(sub == PARTS - 1 - k, wi, down_imag)

    own_read = iota((128, WIDTH), 0) // CHANNEL == iota((128, WIDTH), 1) // STATE
    for k, ref in enumerate((in_re, in_im)):
        wide = jnp.where(own_read, dot(ref[...].reshape(128, STATE), spread, HIGHEST), 0.0)
        top, rest = split(wide)
        drive[0:128, k * WIDTH : (k + 1) * WIDTH] = top
        drive[128:256, k * WIDTH : (k + 1) * WIDTH] = rest
    cr = jnp.where(own_read, dot(out_re[...].reshape(128, STATE), spread, HIGHEST), 0.0)
    ci = jnp.where(own_read, dot(out_im[...].reshape(128, STATE), spread, HIGHEST), 0.0)
    for k, part in enumerate((cr * fr - ci * fi, -(cr * fi + ci * fr))):
        top, rest = split(jnp.transpose(part))
        read[k * WIDTH : (k + 1) * WIDTH, 0:128] = top
        read[k * WIDTH : (k + 1) * WIDTH, 128:256] = rest

    window0 = jnp.where(c == 0, 2, 8)
    p0, p1 = position_of(r0), position_of(r1)
    for k in range(2):
        w = window0 * (k + 1)
        bands[k * ROWS : (k + 1) * ROWS, :] = ((p1 <= p0) & (p1 > p0 - w)).astype(BF16)
        h0, h1 = position_of(iota((ROWS, REACH), 0)), iota((ROWS, REACH), 1) - REACH
        tails[k * ROWS : (k + 1) * ROWS, :] = (h1 > h0 - w).astype(BF16)
    first_head = iota((ROWS, 128), 1) < 64
    here = position_of(iota((ROWS, 128), 0)) + s * ROWS + 1
    recip[...] = 1.0 / jnp.minimum(here, jnp.where(first_head, window0, 2 * window0)).astype(F32)
    last = (position_of(iota((REACH, ROWS), 1)) == iota((REACH, ROWS), 0) + (ROWS - REACH)).astype(BF16)

    pair = (iota((64, 128), 1) % 64 == iota((64, 128), 0)).astype(BF16)
    mixer = jnp.where(
        iota((128, 128), 0) // 64 == iota((128, 128), 1) // 64, dot(mix_raw[...].reshape(128, 64), pair), 0.0
    ).astype(BF16)

    def prepare(p, squares):
        ref = lanes(tok, p, FEATURES)
        f = ref[...].astype(F32)
        lanes(scaled, p, FEATURES)[...] = (f * gain[:, pl.ds(pl.multiple_of(p * FEATURES, 128), FEATURES)]).astype(BF16)
        f = f * f
        return squares + (f[:, 0:128] + f[:, 128:256] + f[:, 256:384])

    squares = prepare(t, jnp.zeros((ROWS, 128), F32))

    events = w_in.events()
    for e in events[0:4]:
        e()
    line.ahead.arrive()
    line.onward.start()
    line.cross_ahead.start()
    line.back.arrive()
    line.cross_back.start()
    for e in events[4:8]:
        e()
    line.own.arrive()
    squares = prepare(line.index["p_own"], squares)
    squares = prepare(line.index["ahead"], squares)
    squares = prepare(line.index["back"], squares)
    line.onward.arrive()
    line.cross_far.start()
    for e in events[8:14]:
        e()
    w_out.begin()
    for move, name in ((line.cross_ahead, "p_ahead"), (line.cross_back, "p_back")):
        move.arrive()
        squares = prepare(line.index[name], squares)
    squares = prepare(line.index["onward"], squares)
    line.cross_far.arrive()
    squares = prepare(line.index["p_onward"], squares)
    inverse = lax.rsqrt(jnp.sum(squares, axis=1, keepdims=True) / 3072.0 + EPSILON)
    events[14]()

    later = w_out.events()
    for e in later[0:4]:
        e()

    entry = (dot(scaled[...], win[...]) * inverse).astype(BF16)
    state_in, pool_in = entry[:, 0:128], entry[:, 128:256]

    push[...] = dot(jnp.concatenate([state_in, state_in], axis=1), drive[...])
    lrb, lib = jnp.broadcast_to(lr, (PARTS, WIDTH)), jnp.broadcast_to(li, (PARTS, WIDTH))

    def advance(j, carry):
        sr, si = carry
        at = pl.ds(pl.multiple_of(j * PARTS, PARTS), PARTS)
        nr = lrb * sr - lib * si + push[at, 0:WIDTH]
        ni = lrb * si + lib * sr + push[at, WIDTH : 2 * WIDTH]
        return nr, ni

    zero = jnp.zeros((PARTS, WIDTH), F32)
    er, ei = lax.fori_loop(0, STEPS, advance, (zero, zero), unroll=8)
    br, bi = times(er, ei, down_real, down_imag)
    br, bi = jnp.sum(br, axis=0, keepdims=True), jnp.sum(bi, axis=0, keepdims=True)
    lines = lambda row: [row[:, 128 * k : 128 * (k + 1)] for k in range(WIDTH // 128)]
    ends[s] = jnp.concatenate(lines(br) + lines(bi), axis=0)
    moves = [
        Move(ends.at[s], ends.at[lax.rem(s - k + PEERS, PEERS)], {"sp": lax.rem(s + k, PEERS)}, (end_send, end_recv), k)
        for k in range(1, PEERS)
    ]
    for m in moves:
        m.start()

    halo[0] = dot(last, pool_in).astype(BF16)
    halo_move = pltpu.make_async_remote_copy(
        src_ref=halo.at[0], dst_ref=halo.at[1], send_sem=halo_send, recv_sem=halo_recv,
        device_id={"sp": lax.rem(s + 1, PEERS)}, device_id_type=MESH)
    halo_move.start()
    for e in later[4:8]:
        e()
    sums = dot(bands[...], pool_in)
    halo_move.wait_recv()
    before = halo[1]
    before = jnp.where(s > 0, before.astype(F32), 0.0).astype(BF16)
    sums = sums + dot(tails[...], before)
    pooled = jnp.where(first_head, sums[0:ROWS], sums[ROWS : 2 * ROWS]) * recip[...] - pool_in.astype(F32)
    top, rest = split(pooled)
    projected = dot(top, mixer) + dot(rest, mixer)
    pool_out = (projected * pool_gain[...]).astype(BF16)
    lanes(pbuf, t, 128)[...] = dot(unsort[...], pool_out).astype(BF16)
    pline = LineGather(lambda p: lanes(pbuf, p, 128), (p_send, p_recv), 0, y, c)
    pline.ahead.start()
    pline.back.start()
    pline.own.start()
    for e in later[8:12]:
        e()

    kr, ki = jnp.where(sub >= 1, pltpu.roll(er, 1, 0), 0.0), jnp.where(sub >= 1, pltpu.roll(ei, 1, 0), 0.0)
    gr, gi = part_real, part_imag
    for hop in (1, 2, 4):
        tr = jnp.where(sub >= hop, pltpu.roll(kr, hop, 0), 0.0)
        ti = jnp.where(sub >= hop, pltpu.roll(ki, hop, 0), 0.0)
        ar, ai = times(tr, ti, gr, gi)
        kr, ki = kr + ar, ki + ai
        gr, gi = times(gr, gi, gr, gi)

    pline.ahead.arrive()
    pline.onward.start()
    pline.cross_ahead.start()
    pline.back.arrive()
    pline.cross_back.start()

    for m in moves:
        m.arrive()
    qr = jnp.concatenate(lines(block_real), axis=0)
    qi = jnp.concatenate(lines(block_imag), axis=0)
    hr, hi = jnp.zeros_like(qr), jnp.zeros_like(qi)
    for q in range(PEERS - 1):
        piece = ends[q]
        ar, ai = times(hr, hi, qr, qi)
        hr, hi = jnp.where(q < s, ar + piece[0:4], hr), jnp.where(q < s, ai + piece[4:8], hi)
    hr = jnp.concatenate([hr[k : k + 1] for k in range(4)], axis=1)
    hi = jnp.concatenate([hi[k : k + 1] for k in range(4)], axis=1)
    ar, ai = times(up_real, up_imag, hr, hi)

    def advance_pair(j, carry):
        one = advance(2 * j, carry)
        two = advance(2 * j + 1, one)
        at = pl.ds(pl.multiple_of(j * 2 * PARTS, 2 * PARTS), 2 * PARTS)
        for k in range(2):
            top, rest = split(jnp.concatenate([one[k], two[k]], axis=0))
            high[at, k * WIDTH : (k + 1) * WIDTH] = top
            low[at, k * WIDTH : (k + 1) * WIDTH] = rest
        return two

    lax.fori_loop(0, STEPS // 2, advance_pair, (kr + ar, ki + ai), unroll=4)
    both = dot(high[...], read[...])
    readout = both[:, 0:128] + both[:, 128:256] + dot(low[...], read[:, 0:128])
    readout = readout + skip_gain[...] * state_in.astype(F32)
    state_out = jax.nn.gelu(readout).astype(BF16)
    lanes(sbuf, t, 128)[...] = dot(unsort[...], state_out).astype(BF16)
    sline = LineGather(lambda p: lanes(sbuf, p, 128), (s_send, s_recv), 0, y, c)
    sline.ahead.start()
    sline.back.start()
    sline.own.start()

    pline.onward.arrive()
    pline.cross_far.start()
    for e in later[12:15]:
        e()
    for m in (pline.own, pline.cross_ahead, pline.cross_back, pline.cross_far):
        m.arrive()
    sline.ahead.arrive()
    sline.onward.start()
    sline.cross_ahead.start()
    sline.back.arrive()
    sline.cross_back.start()
    total = dot(pbuf[...], wpo[...])
    sline.onward.arrive()
    sline.cross_far.start()
    for m in (sline.own, sline.cross_ahead, sline.cross_back, sline.cross_far):
        m.arrive()
    out[...] = (total + dot(sbuf[...], wst[...])).astype(BF16)

    for m in (*line.all, *w_in.all, *w_out.all, *moves, *pline.all, *sline.all):
        m.left()
    halo_move.wait_send()


def body(
    tokens, norm_gain, state_in_weight, pool_in_weight, rate_real, rate_imag, log_step, input_real, input_imag,
    output_real, output_imag, skip_gain, pool_weight, pool_gain, state_out_weight, pool_out_weight,
):
    vmem = pl.BlockSpec(memory_space=pltpu.VMEM)
    dma = pltpu.SemaphoreType.DMA
    return pl.pallas_call(
        kernel,
        out_shape=jax.ShapeDtypeStruct((ROWS, FEATURES), BF16),
        in_specs=[pl.BlockSpec(memory_space=pltpu.HBM)] * 16,
        out_specs=vmem,
        scratch_shapes=[
            pltpu.VMEM((1, 3072), F32),
            pltpu.VMEM((GROUPS, STATE), F32),
            pltpu.VMEM((GROUPS, STATE), F32),
            pltpu.VMEM((1, 64), F32),
            pltpu.VMEM((1, 128), F32),
            pltpu.VMEM((1, 128), F32),
            pltpu.VMEM((ROWS, FEATURES), BF16),
            pltpu.VMEM((ROWS, 3072), BF16),
            pltpu.VMEM((ROWS, 3072), BF16),
            pltpu.VMEM((3072, 256), BF16),
            pltpu.VMEM((1024, FEATURES), BF16),
            pltpu.VMEM((1024, FEATURES), BF16),
            pltpu.VMEM((GROUPS, CHANNEL, STATE), F32),
            pltpu.VMEM((GROUPS, CHANNEL, STATE), F32),
            pltpu.VMEM((GROUPS, CHANNEL, STATE), F32),
            pltpu.VMEM((GROUPS, CHANNEL, STATE), F32),
            pltpu.VMEM((2, 64, 64), BF16),
            pltpu.VMEM((256, 2 * WIDTH), BF16),
            pltpu.VMEM((2 * WIDTH, 256), BF16),
            pltpu.VMEM((ROWS, ROWS), BF16),
            pltpu.VMEM((2 * ROWS, ROWS), BF16),
            pltpu.VMEM((2 * ROWS, REACH), BF16),
            pltpu.VMEM((ROWS, 128), F32),
            pltpu.VMEM((ROWS, 2 * WIDTH), F32),
            pltpu.VMEM((ROWS, 2 * WIDTH), BF16),
            pltpu.VMEM((ROWS, 2 * WIDTH), BF16),
            pltpu.VMEM((PEERS, 8, 128), F32),
            pltpu.VMEM((2, REACH, 128), BF16),
            pltpu.VMEM((ROWS, 1024), BF16),
            pltpu.VMEM((ROWS, 1024), BF16),
            dma((16,)), dma((7,)), dma((7,)), dma((30,)), dma((30,)), dma((30,)), dma((30,)),
            dma((PEERS,)), dma((PEERS,)), dma(()), dma(()), dma((7,)), dma((7,)), dma((7,)), dma((7,)),
        ],
        compiler_params=pltpu.CompilerParams(collective_id=0, has_side_effects=True, vmem_limit_bytes=48 << 20),
    )(
        tokens, norm_gain.reshape(1, 3072), state_in_weight, pool_in_weight, rate_real, rate_imag,
        log_step.reshape(1, 64), jnp.swapaxes(input_real, 1, 2), jnp.swapaxes(input_imag, 1, 2), output_real, output_imag, skip_gain.reshape(1, 1024),
        pool_weight, pool_gain.reshape(1, 1024), state_out_weight, pool_out_weight,
    )


def solution(mesh):
    tile = P("sp", "tp")
    in_specs = (tile, P(), tile, tile, *(P() for _ in range(10)), tile, tile)
    return jax.shard_map(body, mesh=mesh, in_specs=in_specs, out_specs=tile, check_vma=False)
```

time: 150 us -> 63.1 us (0.42)
  Pallas kernels: 0 us -> 49.4 us
  blocking collectives: 30.8 us -> 0 us
  waiting for transfers between devices: 30.1 us -> 0 us
  other arithmetic: 22.2 us -> 0 us
  matrix products: 15.2 us -> 0 us
  between operations: 14.6 us -> 0.03 us
  local copies, waits for them, and re-layouts: 25 us -> 12.8 us
  starting transfers between devices: 10.8 us -> 0 us
    pallas_call x0 -> x1, Pallas kernels: none -> 49.4 us  [body(): pl.pallas_call(kernel, out_shape=jax.ShapeDtypeStruct((ROWS, FEATURES), B...]
    all_gather x4 -> x0, blocking collectives: 30.8 us -> none  [stacked_from(): parts = lax.all_gather(parts, axes[k], axis=0, tiled=True)]
    all_gather x3 -> x0, waiting for transfers between devices: 25 us -> none  [in_one_piece(): result = lax.all_gather(both, axis, axis=dim, tiled=True)]
    dot_general x13 -> x0, matrix products: 15.2 us -> none  [the longest x1 2.64 us: body(): jnp.dot(states_imag, read_matrix_imag, precision=highest)]
    unnamed x64 -> x33, local copies, waits for them, and re-layouts: 0.38 us -> 12.8 us
    reshape x7 -> x0, local copies, waits for them, and re-layouts: 8.02 us -> none  [the longest x1 2.02 us: body(): jnp.einsum('gcn,gh->hngc', local_out_real, group_identity)]
    all_to_all x1 -> x0, starting transfers between devices: 7.26 us -> none  [copy_for_each(): lax.all_to_all(jnp.broadcast_to(array[None], (peers, *array.shape)), axis...]
    all_to_all x1 -> x0, waiting for transfers between devices: 5.02 us -> none  [copy_for_each(): lax.all_to_all(jnp.broadcast_to(array[None], (peers, *array.shape)), axis...]
  transfers between devices with their start and end apart: 5 -> 0, of which waited for: 2 -> 0; matrix products, arithmetic and copies ran while one was open for 38% -> 0% of each run, Pallas kernels for 0% -> 0%
where the time goes in v1:
time: 63.1 us; the launch traced here: 62.3 us
  Pallas kernels  49.4 us (78%)
  local copies, waits for them, and re-layouts  12.8 us (20%)
    pallas_call x1, Pallas kernels, body(): pl.pallas_call(kernel, out_shape=jax.ShapeDtypeStruct((ROWS, FEATURES), B...  49.4 us
    unnamed x33, local copies, waits for them, and re-layouts  12.8 us

profile of v1, /device:TPU:1, one launch (start us, length us, event | category | flops | bytes accessed | tf_op | source)
XLA Modules:
  0.0 62.3 jit_solution(9602152514746656770)
XLA Ops:
  0.0 0.0 copy-start.14
  0.0 0.0 copy-start.13
  0.0 0.0 copy-start.15
  0.0 0.7 %copy-done.14 = f32[1024]{0:T(1024)S(1)} copy-done((f32[1024]{0:T(1024)S(1)}, f32[1024]{0:T(1024)}, u32[]{:S(2)}) %copy-start.14) | copy-done | bytes 4120
  0.7 0.0 copy-done.13
  0.7 0.0 copy-done.15
  0.7 0.0 copy-start
  0.7 1.0 %copy-done = f32[64,64,16]{1,2,0:T(8,128)S(1)} copy-done((f32[64,64,16]{1,2,0:T(8,128)S(1)}, f32[64,64,16]{1,2,0:T(8,128)}, u32[]{:S(2)}) %copy-start) | copy-done | bytes 262168
  1.7 0.0 copy-start.1
  1.8 1.0 %copy-done.1 = f32[64,64,16]{1,2,0:T(8,128)S(1)} copy-done((f32[64,64,16]{1,2,0:T(8,128)S(1)}, f32[64,64,16]{1,2,0:T(8,128)}, u32[]{:S(2)}) %copy-start.1) | copy-done | bytes 262168
  2.8 0.0 copy-start.2
  2.8 1.0 %copy-done.2 = f32[64,16,64]{2,1,0:T(8,128)S(1)} copy-done((f32[64,16,64]{2,1,0:T(8,128)S(1)}, f32[64,16,64]{2,1,0:T(8,128)}, u32[]{:S(2)}) %copy-start.2) | copy-done | bytes 262168
  3.8 0.0 copy-start.3
  3.8 1.0 %copy-done.3 = f32[64,16,64]{2,1,0:T(8,128)S(1)} copy-done((f32[64,16,64]{2,1,0:T(8,128)S(1)}, f32[64,16,64]{2,1,0:T(8,128)}, u32[]{:S(2)}) %copy-start.3) | copy-done | bytes 262168
  4.9 0.0 copy-start.4
  4.9 0.9 %copy-done.4 = bf16[16,64,64]{2,1,0:T(8,128)(2,1)S(1)} copy-done((bf16[16,64,64]{2,1,0:T(8,128)(2,1)S(1)}, bf16[16,64,64]{2,1,0:T(8,128)(2,1)}, u32[]{:S(2)}) %copy-start.4) | copy-done | bytes 131096
  5.8 0.0 copy-start.5
  5.8 0.9 %copy-done.5 = bf16[256,384]{1,0:T(8,128)(2,1)S(1)} copy-done((bf16[256,384]{1,0:T(8,128)(2,1)S(1)}, bf16[256,384]{1,0:T(8,128)(2,1)}, u32[]{:S(2)}) %copy-start.5) | copy-done | bytes 196632
  6.8 0.0 copy-start.6
  6.8 0.8 %copy-done.6 = bf16[192,128]{1,0:T(8,128)(2,1)S(1)} copy-done((bf16[192,128]{1,0:T(8,128)(2,1)S(1)}, bf16[192,128]{1,0:T(8,128)(2,1)}, u32[]{:S(2)}) %copy-start.6) | copy-done | bytes 49176
  7.6 0.0 copy-start.7
  7.6 0.8 %copy-done.7 = bf16[192,128]{1,0:T(8,128)(2,1)S(1)} copy-done((bf16[192,128]{1,0:T(8,128)(2,1)S(1)}, bf16[192,128]{1,0:T(8,128)(2,1)}, u32[]{:S(2)}) %copy-start.7) | copy-done | bytes 49176
  8.4 0.0 copy-start.8
  8.4 0.8 %copy-done.8 = bf16[64,384]{1,0:T(8,128)(2,1)S(1)} copy-done((bf16[64,384]{1,0:T(8,128)(2,1)S(1)}, bf16[64,384]{1,0:T(8,128)(2,1)}, u32[]{:S(2)}) %copy-start.8) | copy-done | bytes 49176
  9.2 0.0 copy-start.9
  9.2 0.8 %copy-done.9 = bf16[64,384]{1,0:T(8,128)(2,1)S(1)} copy-done((bf16[64,384]{1,0:T(8,128)(2,1)S(1)}, bf16[64,384]{1,0:T(8,128)(2,1)}, u32[]{:S(2)}) %copy-start.9) | copy-done | bytes 49176
  9.9 0.0 copy-start.10
  10.0 0.8 %copy-done.10 = f32[64,64]{1,0:T(8,128)S(1)} copy-done((f32[64,64]{1,0:T(8,128)S(1)}, f32[64,64]{1,0:T(8,128)}, u32[]{:S(2)}) %copy-start.10) | copy-done | bytes 16408
  10.7 0.8 %copy-done.11 = f32[64,64]{1,0:T(8,128)S(1)} copy-done((f32[64,64]{1,0:T(8,128)S(1)}, f32[64,64]{1,0:T(8,128)}, u32[]{:S(2)}) %copy-start.11) | copy-done | bytes 16408
  11.5 0.7 %copy-done.12 = f32[3072]{0:T(1024)S(1)} copy-done((f32[3072]{0:T(1024)S(1)}, f32[3072]{0:T(1024)}, u32[]{:S(2)}) %copy-start.12) | copy-done | bytes 12312
  12.2 49.4 %shard_map.154 = bf16[256,384]{1,0:T(8,128)(2,1)S(1)} custom-call(bf16[256,384]{1,0:T(8,128)(2,1)S(1)} %copy-done.5, f32[1,3072]{1,0:T(1,128)S(1)} %bitcast.8, bf16[192,128]{1,0:T(8,128)(2,1)S(1)} %copy-done.6, bf16[192,128]{1,0:T(8,128)(2,1)S(1)} %copy-done.7, f32[64,64]{1,0:T(8,128)S(1)} %copy-done.10, f32[64,64]{1,0:T(8,128)S(1)} %copy-done.11, ...), custom_call_target="tpu_custom_call" | custom-call | tf_op jit(solution)/shard_map/pallas_call | solution.py:452
  61.6 0.7 %copy.18 = bf16[256,384]{1,0:T(8,128)(2,1)} copy(bf16[256,384]{1,0:T(8,128)(2,1)S(1)} %shard_map.154) | data formatting | bytes 393216
  (2 shorter events, 0.0 us)
Async XLA Ops:
  0.0 0.7 %copy-start.14 = (f32[1024]{0:T(1024)S(1)}, f32[1024]{0:T(1024)}, u32[]{:S(2)}) copy-start(f32[1024]{0:T(1024)} %param.29) | copy-start | bytes 12292
  0.0 0.7 %copy-start.13 = (f32[1024]{0:T(1024)S(1)}, f32[1024]{0:T(1024)}, u32[]{:S(2)}) copy-start(f32[1024]{0:T(1024)} %param.27) | copy-start | bytes 12292
  0.0 0.7 %copy-start.15 = (f32[64]{0:T(128)S(1)}, f32[64]{0:T(128)}, u32[]{:S(2)}) copy-start(f32[64]{0:T(128)} %param.22) | copy-start | bytes 772
  0.7 1.0 %copy-start = (f32[64,64,16]{1,2,0:T(8,128)S(1)}, f32[64,64,16]{1,2,0:T(8,128)}, u32[]{:S(2)}) copy-start(f32[64,64,16]{1,2,0:T(8,128)} %param.23) | copy-start | bytes 786436
  1.7 1.0 %copy-start.1 = (f32[64,64,16]{1,2,0:T(8,128)S(1)}, f32[64,64,16]{1,2,0:T(8,128)}, u32[]{:S(2)}) copy-start(f32[64,64,16]{1,2,0:T(8,128)} %param.24) | copy-start | bytes 786436
  2.8 1.0 %copy-start.2 = (f32[64,16,64]{2,1,0:T(8,128)S(1)}, f32[64,16,64]{2,1,0:T(8,128)}, u32[]{:S(2)}) copy-start(f32[64,16,64]{2,1,0:T(8,128)} %output_real.1) | copy-start | bytes 786436
  3.8 1.0 %copy-start.3 = (f32[64,16,64]{2,1,0:T(8,128)S(1)}, f32[64,16,64]{2,1,0:T(8,128)}, u32[]{:S(2)}) copy-start(f32[64,16,64]{2,1,0:T(8,128)} %output_imag.1) | copy-start | bytes 786436
  4.9 0.9 %copy-start.4 = (bf16[16,64,64]{2,1,0:T(8,128)(2,1)S(1)}, bf16[16,64,64]{2,1,0:T(8,128)(2,1)}, u32[]{:S(2)}) copy-start(bf16[16,64,64]{2,1,0:T(8,128)(2,1)} %pool_weight.1) | copy-start | bytes 393220
  5.8 0.9 %copy-start.5 = (bf16[256,384]{1,0:T(8,128)(2,1)S(1)}, bf16[256,384]{1,0:T(8,128)(2,1)}, u32[]{:S(2)}) copy-start(bf16[256,384]{1,0:T(8,128)(2,1)} %tokens.1) | copy-start | bytes 589828
  6.8 0.8 %copy-start.6 = (bf16[192,128]{1,0:T(8,128)(2,1)S(1)}, bf16[192,128]{1,0:T(8,128)(2,1)}, u32[]{:S(2)}) copy-start(bf16[192,128]{1,0:T(8,128)(2,1)} %state_in_w.1) | copy-start | bytes 147460
  7.6 0.8 %copy-start.7 = (bf16[192,128]{1,0:T(8,128)(2,1)S(1)}, bf16[192,128]{1,0:T(8,128)(2,1)}, u32[]{:S(2)}) copy-start(bf16[192,128]{1,0:T(8,128)(2,1)} %pool_in_w.1) | copy-start | bytes 147460
  8.4 0.8 %copy-start.8 = (bf16[64,384]{1,0:T(8,128)(2,1)S(1)}, bf16[64,384]{1,0:T(8,128)(2,1)}, u32[]{:S(2)}) copy-start(bf16[64,384]{1,0:T(8,128)(2,1)} %state_out_w.1) | copy-start | bytes 147460
  9.2 0.8 %copy-start.9 = (bf16[64,384]{1,0:T(8,128)(2,1)S(1)}, bf16[64,384]{1,0:T(8,128)(2,1)}, u32[]{:S(2)}) copy-start(bf16[64,384]{1,0:T(8,128)(2,1)} %pool_out_w.1) | copy-start | bytes 147460
  9.9 0.8 %copy-start.10 = (f32[64,64]{1,0:T(8,128)S(1)}, f32[64,64]{1,0:T(8,128)}, u32[]{:S(2)}) copy-start(f32[64,64]{1,0:T(8,128)} %rate_real_all.1) | copy-start | bytes 49156
  10.7 0.8 %copy-start.11 = (f32[64,64]{1,0:T(8,128)S(1)}, f32[64,64]{1,0:T(8,128)}, u32[]{:S(2)}) copy-start(f32[64,64]{1,0:T(8,128)} %rate_imag_all.1) | copy-start | bytes 49156
  11.5 0.7 %copy-start.12 = (f32[3072]{0:T(1024)S(1)}, f32[3072]{0:T(1024)}, u32[]{:S(2)}) copy-start(f32[3072]{0:T(1024)} %param.17) | copy-start | bytes 36868

commit v2 on v1

--- a/solution.py
+++ b/solution.py
@@ -88,34 +88,38 @@
             self.count += 1
             return move
 
-        def ring(slot, along, e, base):
+        def ring(slot, along, e, base, far):
             v = (lambda k: (base, k)) if along == "x" else (lambda k: (k, base))
             w = (lambda k: (0, k)) if along == "x" else (lambda k: (k, 0))
             return [
                 mk(slot, v(0), v(-e), w(e)),
                 mk(slot, v(0), v(e), w(-e)),
-                mk(slot, v(-e), v(-2 * e), w(e)),
+                mk(slot, v(0), v(2), w(2)) if far else mk(slot, v(-e), v(-2 * e), w(e)),
             ]
 
-        self.a = ring(slot_a, "x", 1, 0)
-        self.b = ring(slot_b, "z", -1, 0)
-        heavy = {0: 1, -1: 1, 1: -1, 2: -1}
-        self.za = {o: ring(slot_a, "z", heavy[o], o) for o in (0, -1, 1, 2)}
-        self.xb = {o: ring(slot_b, "x", -heavy[o], o) for o in (0, -1, 1, 2)}
+        self.a = ring(slot_a, "x", 1, 0, True)
+        self.b = ring(slot_b, "z", -1, 0, True)
+        heavy = {0: 1, -1: -1, 1: -1, 2: 1}
+        self.za = {o: ring(slot_a, "z", heavy[o], o, o == 2) for o in (0, -1, 1, 2)}
+        self.xb = {o: ring(slot_b, "x", -heavy[o], o, o == 2) for o in (0, -1, 1, 2)}
         self.all = [*self.a, *self.b, *(m for r in self.za.values() for m in r), *(m for r in self.xb.values() for m in r)]
 
     def begin(self):
-        for m in (self.a[0], self.a[1], self.b[0], self.b[1], self.za[0][0], self.za[0][1], self.xb[0][0], self.xb[0][1]):
-            m.start()
+        for ring in (self.a, self.b):
+            ring[0].start()
+            ring[1].start()
+        for ring in (self.a, self.b):
+            ring[2].start()
+        for ring in (self.za[0], self.xb[0]):
+            ring[0].start()
+            ring[1].start()
 
     def events(self):
-        def first_of(move, more, ring):
+        def across(move, ring, count):
             def event():
                 move.arrive()
-                if more is not None:
-                    more.start()
-                ring[0].start()
-                ring[1].start()
+                for k in range(count):
+                    ring[k].start()
             return event
 
         def onward(ring):
@@ -126,17 +130,19 @@
 
         def rest():
             for rings in (self.za, self.xb):
-                for o in (0, -1, 1, 2):
+                for o in (0, -1, 1):
                     rings[o][1].arrive()
+                for o in (0, -1, 1):
                     rings[o][2].arrive()
+                for move in rings[2]:
+                    move.arrive()
 
         return [
-            first_of(self.a[0], self.a[2], self.za[-1]), first_of(self.b[0], self.b[2], self.xb[1]),
-            first_of(self.a[1], None, self.za[1]), first_of(self.b[1], None, self.xb[-1]),
+            across(self.a[0], self.za[-1], 2), across(self.b[0], self.xb[1], 2),
+            across(self.a[1], self.za[1], 2), across(self.b[1], self.xb[-1], 2),
+            across(self.a[2], self.za[2], 3), across(self.b[2], self.xb[2], 3),
             onward(self.za[0]), onward(self.xb[0]),
-            first_of(self.a[2], None, self.za[2]), first_of(self.b[2], None, self.xb[2]),
-            onward(self.za[-1]), onward(self.xb[1]), onward(self.za[1]), onward(self.xb[-1]),
-            onward(self.za[2]), onward(self.xb[2]), rest,
+            onward(self.za[-1]), onward(self.xb[1]), onward(self.za[1]), onward(self.xb[-1]), rest,
         ]
 
 
@@ -146,7 +152,7 @@
     gain, rate_real, rate_imag, log_step, skip_gain, pool_gain, own_tokens, tok, scaled, win, wst, wpo, in_re, in_im, out_re, out_im, mix_raw,
     drive, read, unsort, bands, tails, recip, push, high, low, ends, halo, sbuf, pbuf,
     local_sem, tok_send, tok_recv, win_send, win_recv, wout_send, wout_recv,
-    end_send, end_recv, halo_send, halo_recv, s_send, s_recv, p_send, p_recv,
+    ready, end_send, end_recv, halo_send, halo_recv, s_send, s_recv, p_send, p_recv,
 ):
     s, t = lax.axis_index("sp"), lax.axis_index("tp")
     z, x, y, c = s // 4, s % 4, t // 2, t % 2
@@ -181,8 +187,10 @@
         load.start()
 
     barrier = pltpu.get_barrier_semaphore()
-    for k in range(1, PEERS):
-        pl.semaphore_signal(barrier, inc=1, device_id={"sp": lax.rem(s + k, PEERS)}, device_id_type=MESH)
+    beside = [z * 4 + lax.rem(x + k, 4) for k in (1, 2, 3)]
+    above = [lax.rem(z + k, 4) * 4 + x for k in (1, 2, 3)]
+    for peer in (*beside, *above):
+        pl.semaphore_signal(barrier, inc=1, device_id={"sp": peer}, device_id_type=MESH)
     for k in range(1, HEADS_TP):
         pl.semaphore_signal(barrier, inc=1, device_id={"tp": lax.rem(t + k, HEADS_TP)}, device_id_type=MESH)
 
@@ -192,19 +200,30 @@
     lanes(tok, t, FEATURES)[...] = dot(sort, own_tokens[...]).astype(BF16)
     unsort[...] = (position_of(r1) == r0).astype(BF16)
 
-    line = LineGather(lambda p: lanes(tok, p, FEATURES), (tok_send, tok_recv), 0, y, c)
+    def halves(ref, width, sems):
+        def of(k):
+            return lambda p: ref.at[pl.ds(k * 128, 128), pl.ds(pl.multiple_of(p * width, 128), width)]
+        return [LineGather(of(k), sems, 7 * k, y, c) for k in range(2)]
+
+    tok_lines = halves(tok, FEATURES, (tok_send, tok_recv))
     w_in = PlaneGather(
         lambda q: rows(win, q * 192, 96), lambda q: rows(win, q * 192 + 96, 96), (win_send, win_recv), 0, z, x)
     w_out = PlaneGather(
         lambda q: rows(wst, q * 64, 64), lambda q: rows(wpo, q * 64, 64), (wout_send, wout_recv), 0, z, x)
-    for load in loads[1:]:
+    for load in loads[1:3]:
         load.wait()
 
-    pl.semaphore_wait(barrier, PEERS - 1 + HEADS_TP - 1)
-    line.ahead.start()
-    line.back.start()
-    line.own.start()
+    pl.semaphore_wait(barrier, 6 + HEADS_TP - 1)
+    for line in tok_lines:
+        line.ahead.start()
+        line.back.start()
     w_in.begin()
+    for line in tok_lines:
+        line.own.start()
+    for peer in beside:
+        pl.semaphore_signal(ready, inc=1, device_id={"sp": peer}, device_id_type=MESH)
+    for load in loads[3:]:
+        load.wait()
 
     wanted = iota((GROUPS, STATE), 0) + g0
     steps_log = jnp.sum(jnp.where(iota((GROUPS, 64), 1) == wanted, log_step[...], 0.0), axis=1, keepdims=True)
@@ -289,37 +308,48 @@
 
     squares = prepare(t, jnp.zeros((ROWS, 128), F32))
 
+    def relay(line):
+        line.ahead.arrive()
+        line.onward.start()
+        line.cross_ahead.start()
+        line.back.arrive()
+        line.cross_back.start()
+
+    def relay_far(line):
+        line.onward.arrive()
+        line.cross_far.start()
+
     events = w_in.events()
+    one, two = tok_lines
     for e in events[0:4]:
         e()
-    line.ahead.arrive()
-    line.onward.start()
-    line.cross_ahead.start()
-    line.back.arrive()
-    line.cross_back.start()
+    relay(one)
     for e in events[4:8]:
         e()
-    line.own.arrive()
-    squares = prepare(line.index["p_own"], squares)
-    squares = prepare(line.index["ahead"], squares)
-    squares = prepare(line.index["back"], squares)
-    line.onward.arrive()
-    line.cross_far.start()
-    for e in events[8:14]:
+    relay(two)
+    index = one.index
+    for e in events[8:12]:
         e()
     w_out.begin()
-    for move, name in ((line.cross_ahead, "p_ahead"), (line.cross_back, "p_back")):
-        move.arrive()
-        squares = prepare(line.index[name], squares)
-    squares = prepare(line.index["onward"], squares)
-    line.cross_far.arrive()
-    squares = prepare(line.index["p_onward"], squares)
+    relay_far(one)
+    one.own.arrive()
+    two.own.arrive()
+    for name in ("p_own", "ahead", "back"):
+        squares = prepare(index[name], squares)
+    one.cross_ahead.arrive()
+    one.cross_back.arrive()
+    two.cross_ahead.arrive()
+    squares = prepare(index["p_ahead"], squares)
+    two.cross_back.arrive()
+    squares = prepare(index["p_back"], squares)
+    relay_far(two)
+    squares = prepare(index["onward"], squares)
+    one.cross_far.arrive()
+    two.cross_far.arrive()
+    squares = prepare(index["p_onward"], squares)
     inverse = lax.rsqrt(jnp.sum(squares, axis=1, keepdims=True) / 3072.0 + EPSILON)
-    events[14]()
-
+    events[12]()
     later = w_out.events()
-    for e in later[0:4]:
-        e()
 
     entry = (dot(scaled[...], win[...]) * inverse).astype(BF16)
     state_in, pool_in = entry[:, 0:128], entry[:, 128:256]
@@ -344,19 +374,19 @@
         Move(ends.at[s], ends.at[lax.rem(s - k + PEERS, PEERS)], {"sp": lax.rem(s + k, PEERS)}, (end_send, end_recv), k)
         for k in range(1, PEERS)
     ]
+    pl.semaphore_wait(ready, 3)
     for m in moves:
         m.start()
 
-    halo[0] = dot(last, pool_in).astype(BF16)
-    halo_move = pltpu.make_async_remote_copy(
-        src_ref=halo.at[0], dst_ref=halo.at[1], send_sem=halo_send, recv_sem=halo_recv,
-        device_id={"sp": lax.rem(s + 1, PEERS)}, device_id_type=MESH)
+    halo[s] = dot(last, pool_in).astype(BF16)
+    back = lax.rem(s + PEERS - 1, PEERS)
+    halo_move = Move(halo.at[s], halo.at[back], {"sp": lax.rem(s + 1, PEERS)}, (halo_send, halo_recv), 0)
     halo_move.start()
-    for e in later[4:8]:
+    for e in later[0:6]:
         e()
     sums = dot(bands[...], pool_in)
-    halo_move.wait_recv()
-    before = halo[1]
+    halo_move.arrive()
+    before = halo[back]
     before = jnp.where(s > 0, before.astype(F32), 0.0).astype(BF16)
     sums = sums + dot(tails[...], before)
     pooled = jnp.where(first_head, sums[0:ROWS], sums[ROWS : 2 * ROWS]) * recip[...] - pool_in.astype(F32)
@@ -368,8 +398,6 @@
     pline.ahead.start()
     pline.back.start()
     pline.own.start()
-    for e in later[8:12]:
-        e()
 
     kr, ki = jnp.where(sub >= 1, pltpu.roll(er, 1, 0), 0.0), jnp.where(sub >= 1, pltpu.roll(ei, 1, 0), 0.0)
     gr, gi = part_real, part_imag
@@ -380,12 +408,8 @@
         kr, ki = kr + ar, ki + ai
         gr, gi = times(gr, gi, gr, gi)
 
-    pline.ahead.arrive()
-    pline.onward.start()
-    pline.cross_ahead.start()
-    pline.back.arrive()
-    pline.cross_back.start()
-
+    for e in later[6:12]:
+        e()
     for m in moves:
         m.arrive()
     qr = jnp.concatenate(lines(block_real), axis=0)
@@ -410,37 +434,35 @@
         return two
 
     lax.fori_loop(0, STEPS // 2, advance_pair, (kr + ar, ki + ai), unroll=4)
+    relay(pline)
     both = dot(high[...], read[...])
     readout = both[:, 0:128] + both[:, 128:256] + dot(low[...], read[:, 0:128])
     readout = readout + skip_gain[...] * state_in.astype(F32)
     state_out = jax.nn.gelu(readout).astype(BF16)
     lanes(sbuf, t, 128)[...] = dot(unsort[...], state_out).astype(BF16)
-    sline = LineGather(lambda p: lanes(sbuf, p, 128), (s_send, s_recv), 0, y, c)
-    sline.ahead.start()
-    sline.back.start()
-    sline.own.start()
-
-    pline.onward.arrive()
-    pline.cross_far.start()
-    for e in later[12:15]:
-        e()
+    s_lines = halves(sbuf, 128, (s_send, s_recv))
+    for line in s_lines:
+        line.ahead.start()
+        line.back.start()
+    for line in s_lines:
+        line.own.start()
+    relay_far(pline)
+    later[12]()
     for m in (pline.own, pline.cross_ahead, pline.cross_back, pline.cross_far):
         m.arrive()
-    sline.ahead.arrive()
-    sline.onward.start()
-    sline.cross_ahead.start()
-    sline.back.arrive()
-    sline.cross_back.start()
     total = dot(pbuf[...], wpo[...])
-    sline.onward.arrive()
-    sline.cross_far.start()
-    for m in (sline.own, sline.cross_ahead, sline.cross_back, sline.cross_far):
-        m.arrive()
+    for line in s_lines:
+        relay(line)
+    for line in s_lines:
+        relay_far(line)
+    for line in s_lines:
+        for m in (line.own, line.cross_ahead, line.cross_back, line.cross_far):
+            m.arrive()
     out[...] = (total + dot(sbuf[...], wst[...])).astype(BF16)
 
-    for m in (*line.all, *w_in.all, *w_out.all, *moves, *pline.all, *sline.all):
+    for m in (*(m for line in (*tok_lines, *s_lines) for m in line.all), *w_in.all, *w_out.all, *moves, *pline.all):
         m.left()
-    halo_move.wait_send()
+    halo_move.left()
 
 
 def body(
@@ -451,7 +473,7 @@
     dma = pltpu.SemaphoreType.DMA
     return pl.pallas_call(
         kernel,
-        out_shape=jax.ShapeDtypeStruct((ROWS, FEATURES), BF16),
+        out_shape=pltpu.VMEM((ROWS, FEATURES), BF16),
         in_specs=[pl.BlockSpec(memory_space=pltpu.HBM)] * 16,
         out_specs=vmem,
         scratch_shapes=[
@@ -482,18 +504,18 @@
             pltpu.VMEM((ROWS, 2 * WIDTH), BF16),
             pltpu.VMEM((ROWS, 2 * WIDTH), BF16),
             pltpu.VMEM((PEERS, 8, 128), F32),
-            pltpu.VMEM((2, REACH, 128), BF16),
+            pltpu.VMEM((PEERS, REACH, 128), BF16),
             pltpu.VMEM((ROWS, 1024), BF16),
             pltpu.VMEM((ROWS, 1024), BF16),
-            dma((16,)), dma((7,)), dma((7,)), dma((30,)), dma((30,)), dma((30,)), dma((30,)),
-            dma((PEERS,)), dma((PEERS,)), dma(()), dma(()), dma((7,)), dma((7,)), dma((7,)), dma((7,)),
+            dma((16,)), dma((14,)), dma((14,)), dma((30,)), dma((30,)), dma((30,)), dma((30,)),
+            pltpu.SemaphoreType.REGULAR, dma((PEERS,)), dma((PEERS,)), dma((1,)), dma((1,)), dma((14,)), dma((14,)), dma((7,)), dma((7,)),
         ],
-        compiler_params=pltpu.CompilerParams(collective_id=0, has_side_effects=True, vmem_limit_bytes=48 << 20),
-    )(
+        compiler_params=pltpu.CompilerParams(collective_id=0, has_side_effects=True, vmem_limit_bytes=60000000),
+    )(*(pltpu.with_memory_space_constraint(v, pltpu.HBM) for v in (
         tokens, norm_gain.reshape(1, 3072), state_in_weight, pool_in_weight, rate_real, rate_imag,
         log_step.reshape(1, 64), jnp.swapaxes(input_real, 1, 2), jnp.swapaxes(input_imag, 1, 2), output_real, output_imag, skip_gain.reshape(1, 1024),
         pool_weight, pool_gain.reshape(1, 1024), state_out_weight, pool_out_weight,
-    )
+    )))
 
 
 def solution(mesh):

time: 63.1 us -> 45.2 us (0.72); the launches traced: 62.3 us -> 45 us
  local copies, waits for them, and re-layouts: 12.8 us -> 0.68 us
  Pallas kernels: 49.4 us -> 44.4 us
    unnamed x33 -> x1, local copies, waits for them, and re-layouts: 12.8 us -> 0.68 us
    pallas_call x1, Pallas kernels: 49.4 us -> 44.4 us  [body(): pl.pallas_call(kernel, out_shape=pltpu.VMEM((ROWS, FEATURES), BF16), in_s...]
where the time goes in v2:
time: 45.2 us; the launch traced here: 45 us
  Pallas kernels  44.4 us (98%)
  local copies, waits for them, and re-layouts  0.68 us (2%)
    pallas_call x1, Pallas kernels, body(): pl.pallas_call(kernel, out_shape=pltpu.VMEM((ROWS, FEATURES), BF16), in_s...  44.4 us

profile of v2, /device:TPU:1, one launch (start us, length us, event | category | flops | bytes accessed | tf_op | source)
XLA Modules:
  0.0 45.0 jit_solution(585655263576540168)
XLA Ops:
  0.0 44.4 %shard_map.154 = bf16[256,384]{1,0:T(8,128)(2,1)S(1)} custom-call(bf16[256,384]{1,0:T(8,128)(2,1)} %tokens.1, f32[1,3072]{1,0:T(1,128)} %bitcast.8, bf16[192,128]{1,0:T(8,128)(2,1)} %state_in_w.1, bf16[192,128]{1,0:T(8,128)(2,1)} %pool_in_w.1, f32[64,64]{1,0:T(8,128)} %rate_real_all.1, f32[64,64]{1,0:T(8,128)} %rate_imag_all.1, f32[1,64]{1,0:T(1,128)} %bitcast.11, ...), custom_call_target="tpu_custom_call" | custom-call | tf_op jit(solution)/shard_map/pallas_call | solution.py:474
  44.4 0.7 %copy.18 = bf16[256,384]{1,0:T(8,128)(2,1)} copy(bf16[256,384]{1,0:T(8,128)(2,1)S(1)} %shard_map.154) | data formatting | bytes 393216

commit v3 on v2

--- a/solution.py
+++ b/solution.py
@@ -39,31 +39,35 @@
 
 
 class Move:
-    def __init__(self, sends, fills, device, sems, index):
-        self.sends, self.fills, self.device, self.sems, self.index = sends, fills, device, sems, index
-
-    def _copy(self, ref):
+    def __init__(self, sends, fills, device, send_sem, recv_sem):
+        self.sends, self.fills, self.device, self.send_sem, self.recv_sem = sends, fills, device, send_sem, recv_sem
+
+    def copy(self, ref):
         return pltpu.make_async_remote_copy(
-            src_ref=ref, dst_ref=ref, send_sem=self.sems[0].at[self.index], recv_sem=self.sems[1].at[self.index],
+            src_ref=ref, dst_ref=ref, send_sem=self.send_sem, recv_sem=self.recv_sem,
             device_id=self.device, device_id_type=MESH)
 
     def start(self):
-        self._copy(self.sends).start()
+        self.copy(self.sends).start()
 
     def arrive(self):
-        self._copy(self.fills).wait_recv()
-
-    def left(self):
-        self._copy(self.sends).wait_send()
+        self.copy(self.fills).wait_recv()
+
+    def arrive_all(self, ref):
+        self.copy(ref).wait_recv()
+
+    def left_all(self, ref):
+        self.copy(ref).wait_send()
 
 
 class LineGather:
-    def __init__(self, slot, sems, first, y, c):
+    def __init__(self, slot, sems, first, shared, y, c):
         d = 1 - 2 * c
         at = lambda k, core: slot(lax.rem(y + k + 4, 4) * 2 + core)
         to = lambda k, core: {"tp": lax.rem(y + k + 4, 4) * 2 + core}
         o = 1 - c
-        mk = lambda s, f, dev, i: Move(s, f, dev, sems, first + i)
+        places = [first, first + 1, first + 2, shared[0], shared[0], shared[0], shared[1]]
+        mk = lambda s, f, dev, i: Move(s, f, dev, sems[0].at[0], sems[1].at[places[i]])
         self.ahead = mk(at(0, c), at(-d, c), to(d, c), 0)
         self.back = mk(at(0, c), at(d, c), to(-d, c), 1)
         self.onward = mk(at(-d, c), at(-2 * d, c), to(d, c), 2)
@@ -78,31 +82,33 @@
 
 
 class PlaneGather:
-    def __init__(self, slot_a, slot_b, sems, first, z, x):
+    def __init__(self, slot_a, slot_b, sems, nine, z, x):
         wrap = lambda k: lax.rem(k + 4, 4)
         at = lambda dz, dx: wrap(z + dz) * 4 + wrap(x + dx)
-        self.count = 0
-
-        def mk(slot, sent, filled, device):
-            move = Move(slot(at(*sent)), slot(at(*filled)), {"sp": at(*device)}, sems, first + self.count)
-            self.count += 1
-            return move
-
-        def ring(slot, along, e, base, far):
+        self.count, self.nine = 2, nine
+
+        def mk(slot, half, sent, filled, device, shared):
+            place = half if shared else self.count
+            self.count += not shared
+            return Move(slot(at(*sent)), slot(at(*filled)), {"sp": at(*device)}, sems[0].at[half], sems[1].at[place])
+
+        def ring(half, along, e, base, straight, shared):
+            slot = (slot_a, slot_b)[half]
             v = (lambda k: (base, k)) if along == "x" else (lambda k: (k, base))
             w = (lambda k: (0, k)) if along == "x" else (lambda k: (k, 0))
+            third = (v(0), v(2), w(2)) if straight else (v(-e), v(-2 * e), w(e))
             return [
-                mk(slot, v(0), v(-e), w(e)),
-                mk(slot, v(0), v(e), w(-e)),
-                mk(slot, v(0), v(2), w(2)) if far else mk(slot, v(-e), v(-2 * e), w(e)),
+                mk(slot, half, v(0), v(-e), w(e), shared[0]),
+                mk(slot, half, v(0), v(e), w(-e), shared[1]),
+                mk(slot, half, *third, shared[2]),
             ]
 
-        self.a = ring(slot_a, "x", 1, 0, True)
-        self.b = ring(slot_b, "z", -1, 0, True)
+        first, second, last = (False,) * 3, (False, True, True), (True,) * 3
+        self.a = ring(0, "x", 1, 0, True, first)
+        self.b = ring(1, "z", -1, 0, True, first)
         heavy = {0: 1, -1: -1, 1: -1, 2: 1}
-        self.za = {o: ring(slot_a, "z", heavy[o], o, o == 2) for o in (0, -1, 1, 2)}
-        self.xb = {o: ring(slot_b, "x", -heavy[o], o, o == 2) for o in (0, -1, 1, 2)}
-        self.all = [*self.a, *self.b, *(m for r in self.za.values() for m in r), *(m for r in self.xb.values() for m in r)]
+        self.za = {o: ring(0, "z", heavy[o], o, o == 2, last if o == 2 else second) for o in (0, -1, 1, 2)}
+        self.xb = {o: ring(1, "x", -heavy[o], o, o == 2, last if o == 2 else second) for o in (0, -1, 1, 2)}
 
     def begin(self):
         for ring in (self.a, self.b):
@@ -129,13 +135,8 @@
             return event
 
         def rest():
-            for rings in (self.za, self.xb):
-                for o in (0, -1, 1):
-                    rings[o][1].arrive()
-                for o in (0, -1, 1):
-                    rings[o][2].arrive()
-                for move in rings[2]:
-                    move.arrive()
+            self.za[2][0].arrive_all(self.nine[0])
+            self.xb[2][0].arrive_all(self.nine[1])
 
         return [
             across(self.a[0], self.za[-1], 2), across(self.b[0], self.xb[1], 2),
@@ -203,13 +204,15 @@
     def halves(ref, width, sems):
         def of(k):
             return lambda p: ref.at[pl.ds(k * 128, 128), pl.ds(pl.multiple_of(p * width, 128), width)]
-        return [LineGather(of(k), sems, 7 * k, y, c) for k in range(2)]
+        return [LineGather(of(k), sems, 3 * k, (6, 7), y, c) for k in range(2)]
 
     tok_lines = halves(tok, FEATURES, (tok_send, tok_recv))
     w_in = PlaneGather(
-        lambda q: rows(win, q * 192, 96), lambda q: rows(win, q * 192 + 96, 96), (win_send, win_recv), 0, z, x)
+        lambda q: rows(win, q * 192, 96), lambda q: rows(win, q * 192 + 96, 96), (win_send, win_recv),
+        (win.at[0:864], win.at[0:864]), z, x)
     w_out = PlaneGather(
-        lambda q: rows(wst, q * 64, 64), lambda q: rows(wpo, q * 64, 64), (wout_send, wout_recv), 0, z, x)
+        lambda q: rows(wst, q * 64, 64), lambda q: rows(wpo, q * 64, 64), (wout_send, wout_recv),
+        (wst.at[0:576], wpo.at[0:576]), z, x)
     for load in loads[1:3]:
         load.wait()
 
@@ -319,40 +322,41 @@
         line.onward.arrive()
         line.cross_far.start()
 
-    events = w_in.events()
+    events, later = w_in.events(), w_out.events()
     one, two = tok_lines
-    for e in events[0:4]:
-        e()
+    index = one.index
+
+    def run(which, first, last):
+        for e in which[first:last]:
+            e()
+
+    run(events, 0, 4)
     relay(one)
-    for e in events[4:8]:
-        e()
+    run(events, 4, 8)
     relay(two)
-    index = one.index
-    for e in events[8:12]:
-        e()
+    run(events, 8, 12)
     w_out.begin()
     relay_far(one)
-    one.own.arrive()
-    two.own.arrive()
-    for name in ("p_own", "ahead", "back"):
+    for name in ("ahead", "back"):
         squares = prepare(index[name], squares)
-    one.cross_ahead.arrive()
-    one.cross_back.arrive()
-    two.cross_ahead.arrive()
-    squares = prepare(index["p_ahead"], squares)
-    two.cross_back.arrive()
-    squares = prepare(index["p_back"], squares)
     relay_far(two)
     squares = prepare(index["onward"], squares)
-    one.cross_far.arrive()
-    two.cross_far.arrive()
+    one.own.arrive_all(tok.at[:, 0 : 3 * FEATURES])
+    for name in ("p_own", "p_ahead", "p_back"):
+        squares = prepare(index[name], squares)
+    one.cross_far.arrive_all(tok.at[:, 0:FEATURES])
     squares = prepare(index["p_onward"], squares)
     inverse = lax.rsqrt(jnp.sum(squares, axis=1, keepdims=True) / 3072.0 + EPSILON)
     events[12]()
-    later = w_out.events()
 
     entry = (dot(scaled[...], win[...]) * inverse).astype(BF16)
     state_in, pool_in = entry[:, 0:128], entry[:, 128:256]
+
+    pl.semaphore_wait(ready, 3)
+    halo[s] = dot(last, pool_in).astype(BF16)
+    back = lax.rem(s + PEERS - 1, PEERS)
+    halo_move = Move(halo.at[s], halo.at[back], {"sp": lax.rem(s + 1, PEERS)}, halo_send.at[0], halo_recv.at[0])
+    halo_move.start()
 
     push[...] = dot(jnp.concatenate([state_in, state_in], axis=1), drive[...])
     lrb, lib = jnp.broadcast_to(lr, (PARTS, WIDTH)), jnp.broadcast_to(li, (PARTS, WIDTH))
@@ -371,19 +375,13 @@
     lines = lambda row: [row[:, 128 * k : 128 * (k + 1)] for k in range(WIDTH // 128)]
     ends[s] = jnp.concatenate(lines(br) + lines(bi), axis=0)
     moves = [
-        Move(ends.at[s], ends.at[lax.rem(s - k + PEERS, PEERS)], {"sp": lax.rem(s + k, PEERS)}, (end_send, end_recv), k)
+        Move(ends.at[s], ends.at[lax.rem(s - k + PEERS, PEERS)], {"sp": lax.rem(s + k, PEERS)}, end_send.at[0],
+             end_recv.at[0])
         for k in range(1, PEERS)
     ]
-    pl.semaphore_wait(ready, 3)
     for m in moves:
         m.start()
 
-    halo[s] = dot(last, pool_in).astype(BF16)
-    back = lax.rem(s + PEERS - 1, PEERS)
-    halo_move = Move(halo.at[s], halo.at[back], {"sp": lax.rem(s + 1, PEERS)}, (halo_send, halo_recv), 0)
-    halo_move.start()
-    for e in later[0:6]:
-        e()
     sums = dot(bands[...], pool_in)
     halo_move.arrive()
     before = halo[back]
@@ -394,7 +392,7 @@
     projected = dot(top, mixer) + dot(rest, mixer)
     pool_out = (projected * pool_gain[...]).astype(BF16)
     lanes(pbuf, t, 128)[...] = dot(unsort[...], pool_out).astype(BF16)
-    pline = LineGather(lambda p: lanes(pbuf, p, 128), (p_send, p_recv), 0, y, c)
+    pline = LineGather(lambda p: lanes(pbuf, p, 128), (p_send, p_recv), 0, (3, 3), y, c)
     pline.ahead.start()
     pline.back.start()
     pline.own.start()
@@ -408,10 +406,9 @@
         kr, ki = kr + ar, ki + ai
         gr, gi = times(gr, gi, gr, gi)
 
-    for e in later[6:12]:
-        e()
-    for m in moves:
-        m.arrive()
+    run(later, 0, 6)
+    relay(pline)
+    moves[0].arrive_all(ends.at[0 : PEERS - 1])
     qr = jnp.concatenate(lines(block_real), axis=0)
     qi = jnp.concatenate(lines(block_imag), axis=0)
     hr, hi = jnp.zeros_like(qr), jnp.zeros_like(qi)
@@ -434,7 +431,6 @@
         return two
 
     lax.fori_loop(0, STEPS // 2, advance_pair, (kr + ar, ki + ai), unroll=4)
-    relay(pline)
     both = dot(high[...], read[...])
     readout = both[:, 0:128] + both[:, 128:256] + dot(low[...], read[:, 0:128])
     readout = readout + skip_gain[...] * state_in.astype(F32)
@@ -446,23 +442,27 @@
         line.back.start()
     for line in s_lines:
         line.own.start()
+    run(later, 6, 12)
     relay_far(pline)
+    for line in s_lines:
+        relay(line)
+    pline.own.arrive_all(pbuf.at[:, 0:512])
     later[12]()
-    for m in (pline.own, pline.cross_ahead, pline.cross_back, pline.cross_far):
-        m.arrive()
     total = dot(pbuf[...], wpo[...])
     for line in s_lines:
-        relay(line)
-    for line in s_lines:
         relay_far(line)
-    for line in s_lines:
-        for m in (line.own, line.cross_ahead, line.cross_back, line.cross_far):
-            m.arrive()
+    s_lines[0].own.arrive_all(sbuf.at[:, 0 : 3 * 128])
+    s_lines[0].cross_far.arrive_all(sbuf.at[:, 0:128])
     out[...] = (total + dot(sbuf[...], wst[...])).astype(BF16)
 
-    for m in (*(m for line in (*tok_lines, *s_lines) for m in line.all), *w_in.all, *w_out.all, *moves, *pline.all):
-        m.left()
-    halo_move.left()
+    one.own.left_all(tok.at[:, 0 : 7 * FEATURES])
+    for plane, refs in ((w_in, (win.at[0:1440], win.at[0:1440])), (w_out, (wst.at[0:960], wpo.at[0:960]))):
+        plane.a[0].left_all(refs[0])
+        plane.b[0].left_all(refs[1])
+    moves[0].left_all(ends.at[0 : PEERS - 1])
+    pline.own.left_all(pbuf.at[:, 0:896])
+    s_lines[0].own.left_all(sbuf.at[:, 0:896])
+    halo_move.left_all(halo.at[0])
 
 
 def body(
@@ -507,8 +507,9 @@
             pltpu.VMEM((PEERS, REACH, 128), BF16),
             pltpu.VMEM((ROWS, 1024), BF16),
             pltpu.VMEM((ROWS, 1024), BF16),
-            dma((16,)), dma((14,)), dma((14,)), dma((30,)), dma((30,)), dma((30,)), dma((30,)),
-            pltpu.SemaphoreType.REGULAR, dma((PEERS,)), dma((PEERS,)), dma((1,)), dma((1,)), dma((14,)), dma((14,)), dma((7,)), dma((7,)),
+            dma((16,)), dma((1,)), dma((8,)), dma((2,)), dma((14,)), dma((2,)), dma((14,)),
+            pltpu.SemaphoreType.REGULAR, dma((1,)), dma((1,)), dma((1,)), dma((1,)),
+            dma((1,)), dma((8,)), dma((1,)), dma((4,)),
         ],
         compiler_params=pltpu.CompilerParams(collective_id=0, has_side_effects=True, vmem_limit_bytes=60000000),
     )(*(pltpu.with_memory_space_constraint(v, pltpu.HBM) for v in (

time: 45.2 us -> 42.1 us (0.931)
  Pallas kernels: 44.4 us -> 41.3 us
    pallas_call x1, Pallas kernels: 44.4 us -> 41.3 us  [body(): pl.pallas_call(kernel, out_shape=pltpu.VMEM((ROWS, FEATURES), BF16), in_s...]
where the time goes in v3:
time: 42.1 us; the launch traced here: 42 us
  Pallas kernels  41.3 us (98%)
  local copies, waits for them, and re-layouts  0.68 us (2%)
    pallas_call x1, Pallas kernels, body(): pl.pallas_call(kernel, out_shape=pltpu.VMEM((ROWS, FEATURES), BF16), in_s...  41.3 us

profile of v3, /device:TPU:1, one launch (start us, length us, event | category | flops | bytes accessed | tf_op | source)
XLA Modules:
  0.0 42.0 jit_solution(3133233866667768145)
XLA Ops:
  0.0 41.3 %shard_map.154 = bf16[256,384]{1,0:T(8,128)(2,1)S(1)} custom-call(bf16[256,384]{1,0:T(8,128)(2,1)} %tokens.1, f32[1,3072]{1,0:T(1,128)} %bitcast.8, bf16[192,128]{1,0:T(8,128)(2,1)} %state_in_w.1, bf16[192,128]{1,0:T(8,128)(2,1)} %pool_in_w.1, f32[64,64]{1,0:T(8,128)} %rate_real_all.1, f32[64,64]{1,0:T(8,128)} %rate_imag_all.1, f32[1,64]{1,0:T(1,128)} %bitcast.11, ...), custom_call_target="tpu_custom_call" | custom-call | tf_op jit(solution)/shard_map/pallas_call | solution.py:474
  41.3 0.7 %copy.18 = bf16[256,384]{1,0:T(8,128)(2,1)} copy(bf16[256,384]{1,0:T(8,128)(2,1)S(1)} %shard_map.154) | data formatting | bytes 393216

commit v4 on v3

--- a/solution.py
+++ b/solution.py
@@ -61,7 +61,7 @@
 
 
 class LineGather:
-    def __init__(self, slot, sems, first, shared, y, c):
+    def __init__(self, slot, sems, first, shared, y, c, across):
         d = 1 - 2 * c
         at = lambda k, core: slot(lax.rem(y + k + 4, 4) * 2 + core)
         to = lambda k, core: {"tp": lax.rem(y + k + 4, 4) * 2 + core}
@@ -74,7 +74,8 @@
         self.own = mk(at(0, c), at(0, o), to(0, o), 3)
         self.cross_ahead = mk(at(-d, c), at(d, o), to(0, o), 4)
         self.cross_back = mk(at(d, c), at(-d, o), to(0, o), 5)
-        self.cross_far = mk(at(-2 * d, c), at(2 * d, o), to(0, o), 6)
+        self.across = across
+        self.cross_far = mk(at(-d, c) if across else at(-2 * d, c), at(2 * d, o), to(d if across else 0, o), 6)
         self.all = [self.ahead, self.back, self.onward, self.own, self.cross_ahead, self.cross_back, self.cross_far]
         index = lambda k, core: lax.rem(y + k + 4, 4) * 2 + core
         self.index = dict(own=index(0, c), ahead=index(-d, c), back=index(d, c), onward=index(-2 * d, c),
@@ -201,12 +202,12 @@
     lanes(tok, t, FEATURES)[...] = dot(sort, own_tokens[...]).astype(BF16)
     unsort[...] = (position_of(r1) == r0).astype(BF16)
 
-    def halves(ref, width, sems):
+    def halves(ref, width, sems, across):
         def of(k):
             return lambda p: ref.at[pl.ds(k * 128, 128), pl.ds(pl.multiple_of(p * width, 128), width)]
-        return [LineGather(of(k), sems, 3 * k, (6, 7), y, c) for k in range(2)]
-
-    tok_lines = halves(tok, FEATURES, (tok_send, tok_recv))
+        return [LineGather(of(k), sems, 3 * k, (6, 7), y, c, across) for k in range(2)]
+
+    tok_lines = halves(tok, FEATURES, (tok_send, tok_recv), False)
     w_in = PlaneGather(
         lambda q: rows(win, q * 192, 96), lambda q: rows(win, q * 192 + 96, 96), (win_send, win_recv),
         (win.at[0:864], win.at[0:864]), z, x)
@@ -314,13 +315,16 @@
     def relay(line):
         line.ahead.arrive()
         line.onward.start()
+        if line.across:
+            line.cross_far.start()
         line.cross_ahead.start()
         line.back.arrive()
         line.cross_back.start()
 
     def relay_far(line):
         line.onward.arrive()
-        line.cross_far.start()
+        if not line.across:
+            line.cross_far.start()
 
     events, later = w_in.events(), w_out.events()
     one, two = tok_lines
@@ -392,7 +396,7 @@
     projected = dot(top, mixer) + dot(rest, mixer)
     pool_out = (projected * pool_gain[...]).astype(BF16)
     lanes(pbuf, t, 128)[...] = dot(unsort[...], pool_out).astype(BF16)
-    pline = LineGather(lambda p: lanes(pbuf, p, 128), (p_send, p_recv), 0, (3, 3), y, c)
+    pline = LineGather(lambda p: lanes(pbuf, p, 128), (p_send, p_recv), 0, (3, 3), y, c, True)
     pline.ahead.start()
     pline.back.start()
     pline.own.start()
@@ -407,7 +411,6 @@
         gr, gi = times(gr, gi, gr, gi)
 
     run(later, 0, 6)
-    relay(pline)
     moves[0].arrive_all(ends.at[0 : PEERS - 1])
     qr = jnp.concatenate(lines(block_real), axis=0)
     qi = jnp.concatenate(lines(block_imag), axis=0)
@@ -436,16 +439,17 @@
     readout = readout + skip_gain[...] * state_in.astype(F32)
     state_out = jax.nn.gelu(readout).astype(BF16)
     lanes(sbuf, t, 128)[...] = dot(unsort[...], state_out).astype(BF16)
-    s_lines = halves(sbuf, 128, (s_send, s_recv))
+    s_lines = halves(sbuf, 128, (s_send, s_recv), True)
     for line in s_lines:
         line.ahead.start()
         line.back.start()
     for line in s_lines:
         line.own.start()
+    relay(pline)
+    for line in s_lines:
+        relay(line)
     run(later, 6, 12)
     relay_far(pline)
-    for line in s_lines:
-        relay(line)
     pline.own.arrive_all(pbuf.at[:, 0:512])
     later[12]()
     total = dot(pbuf[...], wpo[...])

time: 42.1 us -> 38.8 us (0.922)
  Pallas kernels: 41.3 us -> 38 us
    pallas_call x1, Pallas kernels: 41.3 us -> 38 us  [body(): pl.pallas_call(kernel, out_shape=pltpu.VMEM((ROWS, FEATURES), BF16), in_s...]
where the time goes in v4:
time: 38.8 us; the launch traced here: 38.7 us
  Pallas kernels  38 us (98%)
  local copies, waits for them, and re-layouts  0.68 us (2%)
    pallas_call x1, Pallas kernels, body(): pl.pallas_call(kernel, out_shape=pltpu.VMEM((ROWS, FEATURES), BF16), in_s...  38 us

profile of v4, /device:TPU:1, one launch (start us, length us, event | category | flops | bytes accessed | tf_op | source)
XLA Modules:
  0.0 38.7 jit_solution(2532653945546032701)
XLA Ops:
  0.0 38.0 %shard_map.154 = bf16[256,384]{1,0:T(8,128)(2,1)S(1)} custom-call(bf16[256,384]{1,0:T(8,128)(2,1)} %tokens.1, f32[1,3072]{1,0:T(1,128)} %bitcast.8, bf16[192,128]{1,0:T(8,128)(2,1)} %state_in_w.1, bf16[192,128]{1,0:T(8,128)(2,1)} %pool_in_w.1, f32[64,64]{1,0:T(8,128)} %rate_real_all.1, f32[64,64]{1,0:T(8,128)} %rate_imag_all.1, f32[1,64]{1,0:T(1,128)} %bitcast.11, ...), custom_call_target="tpu_custom_call" | custom-call | tf_op jit(solution)/shard_map/pallas_call | solution.py:478
  38.0 0.7 %copy.18 = bf16[256,384]{1,0:T(8,128)(2,1)} copy(bf16[256,384]{1,0:T(8,128)(2,1)S(1)} %shard_map.154) | data formatting | bytes 393216

commit v5 on v4

--- a/solution.py
+++ b/solution.py
@@ -83,33 +83,43 @@
 
 
 class PlaneGather:
-    def __init__(self, slot_a, slot_b, sems, nine, z, x):
+    def __init__(self, slot_a, slot_b, sems, sized, z, x):
         wrap = lambda k: lax.rem(k + 4, 4)
         at = lambda dz, dx: wrap(z + dz) * 4 + wrap(x + dx)
-        self.count, self.nine = 2, nine
-
-        def mk(slot, half, sent, filled, device, shared):
-            place = half if shared else self.count
-            self.count += not shared
-            return Move(slot(at(*sent)), slot(at(*filled)), {"sp": at(*device)}, sems[0].at[half], sems[1].at[place])
-
-        def ring(half, along, e, base, straight, shared):
+        self.count, self.sized, self.groups, self.places = 0, sized, {}, {}
+
+        def mk(half, sent, filled, device, key=None):
             slot = (slot_a, slot_b)[half]
+            place = self.places.get(key, self.count)
+            if place == self.count:
+                self.count += 1
+            move = Move(slot(at(*sent)), slot(at(*filled)), {"sp": at(*device)}, sems[0].at[half], sems[1].at[place])
+            if key is not None:
+                self.places[key] = place
+                self.groups.setdefault(key, []).append(move)
+            return move
+
+        def ring(half, along, e, base):
             v = (lambda k: (base, k)) if along == "x" else (lambda k: (k, base))
             w = (lambda k: (0, k)) if along == "x" else (lambda k: (k, 0))
-            third = (v(0), v(2), w(2)) if straight else (v(-e), v(-2 * e), w(e))
+            key = lambda k: (half, base if along == "x" else k)
             return [
-                mk(slot, half, v(0), v(-e), w(e), shared[0]),
-                mk(slot, half, v(0), v(e), w(-e), shared[1]),
-                mk(slot, half, *third, shared[2]),
+                mk(half, v(0), v(-e), w(e)),
+                mk(half, v(0), v(e), w(-e), key(e)),
+                mk(half, v(-e), v(-2 * e), w(e), key(2)),
             ]
 
-        first, second, last = (False,) * 3, (False, True, True), (True,) * 3
-        self.a = ring(0, "x", 1, 0, True, first)
-        self.b = ring(1, "z", -1, 0, True, first)
+        self.a = [mk(0, (0, 0), (0, -k), (0, k)) for k in (1, -1, 2)]
+        self.b = [mk(1, (0, 0), (-k, 0), (k, 0)) for k in (-1, 1, 2)]
         heavy = {0: 1, -1: -1, 1: -1, 2: 1}
-        self.za = {o: ring(0, "z", heavy[o], o, o == 2, last if o == 2 else second) for o in (0, -1, 1, 2)}
-        self.xb = {o: ring(1, "x", -heavy[o], o, o == 2, last if o == 2 else second) for o in (0, -1, 1, 2)}
+        self.za = {o: ring(0, "z", heavy[o], o) for o in (0, -1, 1, 2)}
+        self.xb = {o: ring(1, "x", -heavy[o], o) for o in (0, -1, 1, 2)}
+
+    def ready(self, dz):
+        for half in (0, 1):
+            group = self.groups.get((half, dz), [])
+            if group:
+                group[0].arrive_all(self.sized(half, len(group)))
 
     def begin(self):
         for ring in (self.a, self.b):
@@ -135,16 +145,13 @@
                 ring[2].start()
             return event
 
-        def rest():
-            self.za[2][0].arrive_all(self.nine[0])
-            self.xb[2][0].arrive_all(self.nine[1])
-
         return [
             across(self.a[0], self.za[-1], 2), across(self.b[0], self.xb[1], 2),
             across(self.a[1], self.za[1], 2), across(self.b[1], self.xb[-1], 2),
-            across(self.a[2], self.za[2], 3), across(self.b[2], self.xb[2], 3),
+            across(self.a[2], self.za[2], 2), across(self.b[2], self.xb[2], 2),
             onward(self.za[0]), onward(self.xb[0]),
-            onward(self.za[-1]), onward(self.xb[1]), onward(self.za[1]), onward(self.xb[-1]), rest,
+            onward(self.za[-1]), onward(self.xb[1]), onward(self.za[1]), onward(self.xb[-1]),
+            onward(self.za[2]), onward(self.xb[2]),
         ]
 
 
@@ -210,10 +217,10 @@
     tok_lines = halves(tok, FEATURES, (tok_send, tok_recv), False)
     w_in = PlaneGather(
         lambda q: rows(win, q * 192, 96), lambda q: rows(win, q * 192 + 96, 96), (win_send, win_recv),
-        (win.at[0:864], win.at[0:864]), z, x)
+        lambda half, n: win.at[0 : 96 * n], z, x)
     w_out = PlaneGather(
         lambda q: rows(wst, q * 64, 64), lambda q: rows(wpo, q * 64, 64), (wout_send, wout_recv),
-        (wst.at[0:576], wpo.at[0:576]), z, x)
+        lambda half, n: (wst, wpo)[half].at[0 : 64 * n], z, x)
     for load in loads[1:3]:
         load.wait()
 
@@ -338,7 +345,7 @@
     relay(one)
     run(events, 4, 8)
     relay(two)
-    run(events, 8, 12)
+    run(events, 8, 14)
     w_out.begin()
     relay_far(one)
     for name in ("ahead", "back"):
@@ -351,9 +358,16 @@
     one.cross_far.arrive_all(tok.at[:, 0:FEATURES])
     squares = prepare(index["p_onward"], squares)
     inverse = lax.rsqrt(jnp.sum(squares, axis=1, keepdims=True) / 3072.0 + EPSILON)
-    events[12]()
-
-    entry = (dot(scaled[...], win[...]) * inverse).astype(BF16)
+
+    def row_part(ref, dz, width, axis):
+        at = pl.ds(pl.multiple_of(lax.rem(z + dz + 4, 4) * width, 128), width)
+        return ref[:, at] if axis else ref[at, :]
+
+    product = jnp.zeros((ROWS, 256), F32)
+    for dz in (0, 1, -1, 2):
+        w_in.ready(dz)
+        product = product + dot(row_part(scaled, dz, 768, 1), row_part(win, dz, 768, 0))
+    entry = (product * inverse).astype(BF16)
     state_in, pool_in = entry[:, 0:128], entry[:, 128:256]
 
     pl.semaphore_wait(ready, 3)
@@ -448,16 +462,23 @@
     relay(pline)
     for line in s_lines:
         relay(line)
-    run(later, 6, 12)
+    run(later, 6, 14)
     relay_far(pline)
     pline.own.arrive_all(pbuf.at[:, 0:512])
-    later[12]()
-    total = dot(pbuf[...], wpo[...])
+    total = jnp.zeros((ROWS, FEATURES), F32)
+    for dz in (0, 1, -1):
+        w_out.ready(dz)
+        total = total + dot(row_part(pbuf, dz, 256, 1), row_part(wpo, dz, 256, 0))
     for line in s_lines:
         relay_far(line)
     s_lines[0].own.arrive_all(sbuf.at[:, 0 : 3 * 128])
     s_lines[0].cross_far.arrive_all(sbuf.at[:, 0:128])
-    out[...] = (total + dot(sbuf[...], wst[...])).astype(BF16)
+    for dz in (0, 1, -1):
+        total = total + dot(row_part(sbuf, dz, 256, 1), row_part(wst, dz, 256, 0))
+    w_out.ready(2)
+    total = total + dot(row_part(pbuf, 2, 256, 1), row_part(wpo, 2, 256, 0))
+    total = total + dot(row_part(sbuf, 2, 256, 1), row_part(wst, 2, 256, 0))
+    out[...] = total.astype(BF16)
 
     one.own.left_all(tok.at[:, 0 : 7 * FEATURES])
     for plane, refs in ((w_in, (win.at[0:1440], win.at[0:1440])), (w_out, (wst.at[0:960], wpo.at[0:960]))):
@@ -511,7 +532,7 @@
             pltpu.VMEM((PEERS, REACH, 128), BF16),
             pltpu.VMEM((ROWS, 1024), BF16),
             pltpu.VMEM((ROWS, 1024), BF16),
-            dma((16,)), dma((1,)), dma((8,)), dma((2,)), dma((14,)), dma((2,)), dma((14,)),
+            dma((16,)), dma((1,)), dma((8,)), dma((2,)), dma((24,)), dma((2,)), dma((24,)),
             pltpu.SemaphoreType.REGULAR, dma((1,)), dma((1,)), dma((1,)), dma((1,)),
             dma((1,)), dma((8,)), dma((1,)), dma((4,)),
         ],

time: 38.8 us -> 37.7 us (0.972)
  Pallas kernels: 38 us -> 36.9 us
    pallas_call x1, Pallas kernels: 38 us -> 36.9 us  [body(): pl.pallas_call(kernel, out_shape=pltpu.VMEM((ROWS, FEATURES), BF16), in_s...]
where the time goes in v5:
time: 37.7 us; the launch traced here: 37.6 us
  Pallas kernels  36.9 us (98%)
  local copies, waits for them, and re-layouts  0.68 us (2%)
    pallas_call x1, Pallas kernels, body(): pl.pallas_call(kernel, out_shape=pltpu.VMEM((ROWS, FEATURES), BF16), in_s...  36.9 us

profile of v5, /device:TPU:1, one launch (start us, length us, event | category | flops | bytes accessed | tf_op | source)
XLA Modules:
  0.0 37.6 jit_solution(844028954841126935)
XLA Ops:
  0.0 36.9 %shard_map.154 = bf16[256,384]{1,0:T(8,128)(2,1)S(1)} custom-call(bf16[256,384]{1,0:T(8,128)(2,1)} %tokens.1, f32[1,3072]{1,0:T(1,128)} %bitcast.8, bf16[192,128]{1,0:T(8,128)(2,1)} %state_in_w.1, bf16[192,128]{1,0:T(8,128)(2,1)} %pool_in_w.1, f32[64,64]{1,0:T(8,128)} %rate_real_all.1, f32[64,64]{1,0:T(8,128)} %rate_imag_all.1, f32[1,64]{1,0:T(1,128)} %bitcast.11, ...), custom_call_target="tpu_custom_call" | custom-call | tf_op jit(solution)/shard_map/pallas_call | solution.py:499
  36.9 0.7 %copy.18 = bf16[256,384]{1,0:T(8,128)(2,1)} copy(bf16[256,384]{1,0:T(8,128)(2,1)S(1)} %shard_map.154) | data formatting | bytes 393216

commit v6 on v5

--- a/solution.py
+++ b/solution.py
@@ -221,13 +221,12 @@
     w_out = PlaneGather(
         lambda q: rows(wst, q * 64, 64), lambda q: rows(wpo, q * 64, 64), (wout_send, wout_recv),
         lambda half, n: (wst, wpo)[half].at[0 : 64 * n], z, x)
-    for load in loads[1:3]:
-        load.wait()
-
     pl.semaphore_wait(barrier, 6 + HEADS_TP - 1)
     for line in tok_lines:
         line.ahead.start()
         line.back.start()
+    for load in loads[1:3]:
+        load.wait()
     w_in.begin()
     for line in tok_lines:
         line.own.start()
@@ -392,10 +391,12 @@
     br, bi = jnp.sum(br, axis=0, keepdims=True), jnp.sum(bi, axis=0, keepdims=True)
     lines = lambda row: [row[:, 128 * k : 128 * (k + 1)] for k in range(WIDTH // 128)]
     ends[s] = jnp.concatenate(lines(br) + lines(bi), axis=0)
+    block = lambda dz, dx: lax.rem(z + dz + 4, 4) * 4 + lax.rem(x + dx + 4, 4)
+    offsets = [(dz, dx) for dz in (2, 1, -1, 0) for dx in (2, 1, -1, 0)][:-1]
+    farthest_first = sorted(offsets, key=lambda o: -abs(o[0]) - abs(o[1]))
     moves = [
-        Move(ends.at[s], ends.at[lax.rem(s - k + PEERS, PEERS)], {"sp": lax.rem(s + k, PEERS)}, end_send.at[0],
-             end_recv.at[0])
-        for k in range(1, PEERS)
+        Move(ends.at[s], ends.at[block(-dz, -dx)], {"sp": block(dz, dx)}, end_send.at[0], end_recv.at[0])
+        for dz, dx in farthest_first
     ]
     for m in moves:
         m.start()

time: 37.7 us -> 37.7 us (level)
  no operation moved by 1% of the time
where the time goes in v6:
time: 37.7 us; the launch traced here: 37.5 us
  Pallas kernels  36.8 us (98%)
  local copies, waits for them, and re-layouts  0.68 us (2%)
    pallas_call x1, Pallas kernels, body(): pl.pallas_call(kernel, out_shape=pltpu.VMEM((ROWS, FEATURES), BF16), in_s...  36.8 us

profile of v6, /device:TPU:1, one launch (start us, length us, event | category | flops | bytes accessed | tf_op | source)
XLA Modules:
  0.0 37.5 jit_solution(6038327513492509130)
XLA Ops:
  0.0 36.8 %shard_map.154 = bf16[256,384]{1,0:T(8,128)(2,1)S(1)} custom-call(bf16[256,384]{1,0:T(8,128)(2,1)} %tokens.1, f32[1,3072]{1,0:T(1,128)} %bitcast.8, bf16[192,128]{1,0:T(8,128)(2,1)} %state_in_w.1, bf16[192,128]{1,0:T(8,128)(2,1)} %pool_in_w.1, f32[64,64]{1,0:T(8,128)} %rate_real_all.1, f32[64,64]{1,0:T(8,128)} %rate_imag_all.1, f32[1,64]{1,0:T(1,128)} %bitcast.11, ...), custom_call_target="tpu_custom_call" | custom-call | tf_op jit(solution)/shard_map/pallas_call | solution.py:500
  36.9 0.7 %copy.18 = bf16[256,384]{1,0:T(8,128)(2,1)} copy(bf16[256,384]{1,0:T(8,128)(2,1)S(1)} %shard_map.154) | data formatting | bytes 393216

commit v7 on v6

--- a/solution.py
+++ b/solution.py
@@ -209,12 +209,13 @@
     lanes(tok, t, FEATURES)[...] = dot(sort, own_tokens[...]).astype(BF16)
     unsort[...] = (position_of(r1) == r0).astype(BF16)
 
-    def halves(ref, width, sems, across):
+    def halves(ref, width, sems, across, count):
         def of(k):
-            return lambda p: ref.at[pl.ds(k * 128, 128), pl.ds(pl.multiple_of(p * width, 128), width)]
-        return [LineGather(of(k), sems, 3 * k, (6, 7), y, c, across) for k in range(2)]
-
-    tok_lines = halves(tok, FEATURES, (tok_send, tok_recv), False)
+            size = ROWS // count
+            return lambda p: ref.at[pl.ds(k * size, size), pl.ds(pl.multiple_of(p * width, 128), width)]
+        return [LineGather(of(k), sems, 3 * k, (3 * count, 3 * count + 1), y, c, across) for k in range(count)]
+
+    tok_lines = halves(tok, FEATURES, (tok_send, tok_recv), False, 4)
     w_in = PlaneGather(
         lambda q: rows(win, q * 192, 96), lambda q: rows(win, q * 192 + 96, 96), (win_send, win_recv),
         lambda half, n: win.at[0 : 96 * n], z, x)
@@ -333,7 +334,7 @@
             line.cross_far.start()
 
     events, later = w_in.events(), w_out.events()
-    one, two = tok_lines
+    one, two, three, four = tok_lines
     index = one.index
 
     def run(which, first, last):
@@ -342,14 +343,18 @@
 
     run(events, 0, 4)
     relay(one)
-    run(events, 4, 8)
+    run(events, 4, 6)
     relay(two)
+    run(events, 6, 8)
+    relay(three)
+    relay(four)
     run(events, 8, 14)
     w_out.begin()
-    relay_far(one)
+    for line in (one, two, three):
+        relay_far(line)
     for name in ("ahead", "back"):
         squares = prepare(index[name], squares)
-    relay_far(two)
+    relay_far(four)
     squares = prepare(index["onward"], squares)
     one.own.arrive_all(tok.at[:, 0 : 3 * FEATURES])
     for name in ("p_own", "p_ahead", "p_back"):
@@ -454,7 +459,7 @@
     readout = readout + skip_gain[...] * state_in.astype(F32)
     state_out = jax.nn.gelu(readout).astype(BF16)
     lanes(sbuf, t, 128)[...] = dot(unsort[...], state_out).astype(BF16)
-    s_lines = halves(sbuf, 128, (s_send, s_recv), True)
+    s_lines = halves(sbuf, 128, (s_send, s_recv), True, 2)
     for line in s_lines:
         line.ahead.start()
         line.back.start()
@@ -533,7 +538,7 @@
             pltpu.VMEM((PEERS, REACH, 128), BF16),
             pltpu.VMEM((ROWS, 1024), BF16),
             pltpu.VMEM((ROWS, 1024), BF16),
-            dma((16,)), dma((1,)), dma((8,)), dma((2,)), dma((24,)), dma((2,)), dma((24,)),
+            dma((16,)), dma((1,)), dma((16,)), dma((2,)), dma((24,)), dma((2,)), dma((24,)),
             pltpu.SemaphoreType.REGULAR, dma((1,)), dma((1,)), dma((1,)), dma((1,)),
             dma((1,)), dma((8,)), dma((1,)), dma((4,)),
         ],

time: 37.7 us -> 37.7 us (level)
  no operation moved by 1% of the time
where the time goes in v7:
time: 37.7 us; the launch traced here: 37.6 us
  Pallas kernels  36.9 us (98%)
  local copies, waits for them, and re-layouts  0.68 us (2%)
    pallas_call x1, Pallas kernels, body(): pl.pallas_call(kernel, out_shape=pltpu.VMEM((ROWS, FEATURES), BF16), in_s...  36.9 us

profile of v7, /device:TPU:1, one launch (start us, length us, event | category | flops | bytes accessed | tf_op | source)
XLA Modules:
  0.0 37.6 jit_solution(9959864941889322200)
XLA Ops:
  0.0 36.9 %shard_map.154 = bf16[256,384]{1,0:T(8,128)(2,1)S(1)} custom-call(bf16[256,384]{1,0:T(8,128)(2,1)} %tokens.1, f32[1,3072]{1,0:T(1,128)} %bitcast.8, bf16[192,128]{1,0:T(8,128)(2,1)} %state_in_w.1, bf16[192,128]{1,0:T(8,128)(2,1)} %pool_in_w.1, f32[64,64]{1,0:T(8,128)} %rate_real_all.1, f32[64,64]{1,0:T(8,128)} %rate_imag_all.1, f32[1,64]{1,0:T(1,128)} %bitcast.11, ...), custom_call_target="tpu_custom_call" | custom-call | tf_op jit(solution)/shard_map/pallas_call | solution.py:505
  36.9 0.7 %copy.18 = bf16[256,384]{1,0:T(8,128)(2,1)} copy(bf16[256,384]{1,0:T(8,128)(2,1)S(1)} %shard_map.154) | data formatting | bytes 393216
